TPU v7x, 256 devices: a whole 4x4x8 slice. The times are simulated.
256 devices in a mesh: sp: 64 (over z, y, core), tp: 4 (over x).
Axes of the slice: x: 4, y: 4, z: 8, core: 2. Of those that a mesh axis runs over, the one named last changes fastest.
Arguments:
- tokens: bfloat16 [16384, 2048], P('sp', 'tp'), may hold values from -6 to 6
- in_gain: float32 [2048], replicated, may hold values from 0.1 to 1.9
- query_down: bfloat16 [2048, 512], replicated, may hold values from -0.125 to 0.125
- latent_down: bfloat16 [2048, 256], replicated, may hold values from -0.125 to 0.125
- rope_down: bfloat16 [2048, 32], replicated, may hold values from -0.125 to 0.125
- query_gain: float32 [512], replicated, may hold values from 0.5 to 12
- latent_gain: float32 [256], replicated, may hold values from 0.5 to 12
- query_nope: bfloat16 [512, 1024], P(None, 'tp'), may hold values from -0.25 to 0.25
- query_rope: bfloat16 [512, 512], P(None, 'tp'), may hold values from -0.25 to 0.25
- key_up: bfloat16 [256, 1024], P(None, 'tp'), may hold values from -0.375 to 0.375
- value_up: bfloat16 [256, 1024], P(None, 'tp'), may hold values from -0.375 to 0.375
- conv_value: bfloat16 [2048, 2048], P(None, 'tp'), may hold values from -0.125 to 0.125
- conv_gate: bfloat16 [2048, 2048], P(None, 'tp'), may hold values from -0.125 to 0.125
- conv_taps: float32 [31, 2048], P(None, 'tp'), may hold values from -1 to 1
- conv_bias: float32 [2048], P('tp'), may hold values from 0.05 to 2.25
- channel_gain: float32 [2048], P('tp'), may hold values from 0.1 to 1.9
- out_attend: bfloat16 [1024, 2048], P('tp'), may hold values from -0.109375 to 0.109375
- out_conv: bfloat16 [2048, 2048], P('tp'), may hold values from -0.109375 to 0.109375
Outputs:
- mixed: bfloat16 [16384, 2048], P('sp', 'tp')
All inputs are finite; a program needn't handle non-finite values.
Results may differ from a plain program's by a relative error of at most 0.013.
The roundings to bfloat16 on the way count: a program that leaves them out, or rounds other values in their place, can miss the bound.
Values may be sent and summed in bfloat16 or wider, within the bound.
No kernel may reach another device: no remote copies, remote signals or barrier semaphores. Data moves between devices by JAX's collectives and lax.ppermute only.
A program may use at most 128 MiB of HBM per device.

v0:
```python
import math

import jax
import jax.numpy as jnp
from jax import lax
from jax.sharding import PartitionSpec as P

eps_norm = 1e-06
eps_layer = 1e-05
theta = 10000.0


def laid_out(blocks, dim):
    dims = list(blocks.shape[1:])
    dims[dim] *= blocks.shape[0]
    return jnp.moveaxis(blocks, 0, dim).reshape(dims)


def sent_to_all(shard, axis):
    copies = jnp.broadcast_to(shard, (lax.axis_size(axis), *shard.shape))
    return lax.all_to_all(copies, axis, split_axis=0, concat_axis=0, tiled=True)


def gather_directly(shard, axis, dim):
    return laid_out(sent_to_all(shard, axis), dim)


def sent_together(arrays, axis, dim, along):
    ends, at = ([], 0)
    for a in arrays[:-1]:
        at += a.shape[along]
        ends.append(at)
    both = jnp.concatenate(arrays, axis=along)
    return tuple(jnp.split(lax.all_gather(both, axis, axis=dim, tiled=True), ends, axis=along))


def padded_2(cells, sides, width):
    for axis, dim in sides:
        count = lax.axis_size(axis)
        ends = count - 1
        head = lax.slice_in_dim(cells, 0, width, axis=dim)
        tail = lax.slice_in_dim(cells, cells.shape[dim] - width, cells.shape[dim], axis=dim)
        cells = jnp.concatenate(
            [
                lax.ppermute(tail, axis, [(i, (i + 1) % count) for i in range(ends)]),
                cells,
                lax.ppermute(head, axis, [((i + 1) % count, i) for i in range(ends)]),
            ],
            axis=dim,
        )
    return cells


def over_copies(shard, axis):
    return sent_to_all(shard, axis).sum(axis=0)


def cut_along(shard, dim, peers):
    dims = shard.shape
    blocks = shard.reshape(*dims[:dim], peers, dims[dim] // peers, *dims[dim + 1 :])
    return jnp.moveaxis(blocks, dim, 0)


def sum_at_owner(shard, axis, dim):
    blocks = cut_along(shard, dim, lax.axis_size(axis))
    arrived = lax.all_to_all(blocks, axis, split_axis=0, concat_axis=0, tiled=True)
    return arrived.astype(jnp.float32).sum(axis=0)


def rms_scale(values, gain):
    return values * lax.rsqrt(jnp.mean(values * values, axis=-1, keepdims=True) + eps_norm) * gain


def rotate(values, positions):
    half = values.shape[-1] // 2
    freqs = theta ** (-jnp.arange(half).astype(jnp.float32) / half)
    angles = positions[..., None] * freqs
    cosine = jnp.cos(angles)
    sine = jnp.sin(angles)
    first = values[..., :half]
    second = values[..., half:]
    return jnp.concatenate(
        [first * cosine - second * sine, second * cosine + first * sine], axis=-1
    )


def attend_block(state, q_heads, r_heads, k_nope, values, rope_key):
    highest, total, weighted = state
    heads = q_heads.shape[1]
    key_heads = k_nope.reshape(k_nope.shape[0], heads, -1)
    value_heads = values.reshape(values.shape[0], heads, -1)
    score_scale = (q_heads.shape[2] + r_heads.shape[2]) ** (-0.5)
    scores = (
        jnp.einsum("qhd,khd->hqk", q_heads, key_heads, preferred_element_type=jnp.float32)
        + jnp.einsum("qhd,kd->hqk", r_heads, rope_key, preferred_element_type=jnp.float32)
    ) * score_scale
    new_high = jnp.maximum(highest, jnp.max(scores, axis=-1))
    factor = jnp.exp(highest - new_high)
    weight = jnp.exp(scores - new_high[..., None])
    total = total * factor + jnp.sum(weight, axis=-1)
    weighted = weighted * factor[..., None] + jnp.einsum(
        "hqk,khd->hqd", weight.astype(jnp.bfloat16), value_heads, preferred_element_type=jnp.float32
    )
    return (new_high, total, weighted)


def over_blocks(state, arrays, step):
    count = arrays[0].shape[0]
    size = math.gcd(count, 1024)
    shaped = tuple((item.reshape((count // size, size) + item.shape[1:]) for item in arrays))

    def one_block(carry, block):
        return (step(carry, block), None)

    state, unused = lax.scan(one_block, state, shaped)
    return state


def per_device(
    tokens,
    in_gain,
    query_down,
    latent_down,
    rope_down,
    query_gain,
    latent_gain,
    query_nope,
    query_rope,
    key_up,
    value_up,
    conv_value,
    conv_gate,
    conv_taps,
    conv_bias,
    channel_gain,
    out_attend,
    out_conv,
):
    row_count = tokens.shape[0]
    width = in_gain.shape[0]
    local_ch = conv_value.shape[1]
    positions = (lax.axis_index("sp") * row_count + jnp.arange(row_count)).astype(jnp.float32)
    piece_f = gather_directly(tokens, "tp", 1).astype(jnp.float32)
    scaled = (piece_f * in_gain).astype(jnp.bfloat16)

    def add_rows(weight):
        return jnp.dot(scaled, weight, preferred_element_type=jnp.float32)

    square_sum = jnp.sum(piece_f * piece_f, axis=1)
    q_pre = add_rows(query_down)
    kv_pre = add_rows(latent_down)
    rope_pre = add_rows(rope_down)
    value_pre = add_rows(conv_value)
    gate_pre = add_rows(conv_gate)
    row_scale = lax.rsqrt(square_sum / width + eps_norm)[:, None]
    q_latent = rms_scale(row_scale * q_pre, query_gain).astype(jnp.bfloat16)
    kv_latent = rms_scale(row_scale * kv_pre, latent_gain).astype(jnp.bfloat16)
    rope_key = rotate(row_scale * rope_pre, positions).astype(jnp.bfloat16)
    rope_size = rope_down.shape[1]
    heads = query_rope.shape[1] // rope_size
    q_heads = (
        jnp.dot(q_latent, query_nope, preferred_element_type=jnp.float32)
        .astype(jnp.bfloat16)
        .reshape(row_count, heads, -1)
    )
    q_turn = jnp.dot(q_latent, query_rope, preferred_element_type=jnp.float32).reshape(
        row_count, heads, rope_size
    )
    r_heads = rotate(q_turn, positions[:, None]).astype(jnp.bfloat16)
    value_size = value_up.shape[1] // heads
    start_state = (
        jnp.full((heads, row_count), -jnp.inf, jnp.float32),
        jnp.zeros((heads, row_count), jnp.float32),
        jnp.zeros((heads, row_count, value_size), jnp.float32),
    )
    own_keys = jnp.dot(kv_latent, key_up, preferred_element_type=jnp.float32).astype(jnp.bfloat16)
    own_values = jnp.dot(kv_latent, value_up, preferred_element_type=jnp.float32).astype(
        jnp.bfloat16
    )

    def head_step(state, block):
        return attend_block(state, q_heads, r_heads, block[0], block[1], block[2])

    highest, total, weighted = over_blocks(
        start_state, sent_together((own_keys, own_values, rope_key), "sp", 0, 1), head_step
    )
    attended = jnp.transpose((weighted / total[..., None]).astype(jnp.bfloat16), (1, 0, 2)).reshape(
        row_count, heads * value_size
    )
    glu = (row_scale * value_pre * jax.nn.sigmoid(row_scale * gate_pre)).astype(jnp.bfloat16)
    taps = conv_taps.shape[0]
    padded = padded_2(glu, (("sp", 0),), taps // 2).astype(jnp.float32)
    conv = jnp.zeros((row_count, local_ch), jnp.float32) + conv_bias
    for tap in range(taps):
        conv = conv + conv_taps[tap] * padded[tap : tap + row_count]
    channels = local_ch * lax.axis_size("tp")
    mean = over_copies(jnp.sum(conv, axis=-1), "tp")[:, None] / channels
    centred = conv - mean
    spread = over_copies(jnp.sum(centred * centred, axis=-1), "tp")[:, None] / channels
    activated = jax.nn.silu(centred * lax.rsqrt(spread + eps_layer) * channel_gain).astype(
        jnp.bfloat16
    )
    contract = (((0,), (1,)), ((), ()))
    summed = sum_at_owner(
        (
            lax.dot_general(out_attend, attended, contract, preferred_element_type=jnp.float32)
            + lax.dot_general(out_conv, activated, contract, preferred_element_type=jnp.float32)
        ).astype(jnp.bfloat16),
        "tp",
        0,
    )
    return jnp.transpose(summed).astype(jnp.bfloat16)


def solution(mesh):
    in_specs = (
        P("sp", "tp"),
        P(),
        P(),
        P(),
        P(),
        P(),
        P(),
        P(None, "tp"),
        P(None, "tp"),
        P(None, "tp"),
        P(None, "tp"),
        P(None, "tp"),
        P(None, "tp"),
        P(None, "tp"),
        P("tp"),
        P("tp"),
        P("tp", None),
        P("tp", None),
    )
    out_specs = P("sp", "tp")
    return jax.shard_map(
        per_device, mesh=mesh, in_specs=in_specs, out_specs=out_specs, check_vma=False
    )
```

profile of v0, /device:TPU:1, one launch (start us, length us, event | category | flops | bytes accessed | tf_op | source)
XLA Modules:
  0.0 269.6 jit_solution(14440085917408073910)
XLA Ops:
  8.8 5.0 %all-to-all-start = ((bf16[4,256,512]{1,2,0:T(8,128)(2,1)}), bf16[4,256,512]{1,2,0:T(8,128)(2,1)S(1)}, u32[]{:S(2)}, u32[]{:S(2)}) async-start(bf16[4,256,512]{1,2,0:T(8,128)(2,1)} %broadcast_in_dim.17), calls=%async_computation | async-start | bytes 2097152 | tf_op jit(solution)/shard_map/all_to_all | solution.py:21
  13.8 13.3 %all-to-all-done = bf16[4,256,512]{1,2,0:T(8,128)(2,1)S(1)} async-done(((bf16[4,256,512]{1,2,0:T(8,128)(2,1)}), bf16[4,256,512]{1,2,0:T(8,128)(2,1)S(1)}, u32[]{:S(2)}, u32[]{:S(2)}) %all-to-all-start) | async-done | bytes 1048608 | tf_op jit(solution)/shard_map/all_to_all | solution.py:21
  34.1 2.9 %fusion.18 = f32[256,512]{1,0:T(8,128)S(1)} fusion(bf16[256,2048]{0,1:T(8,128)(2,1)} %copy-done.1, bf16[2048,512]{1,0:T(8,128)(2,1)} %param.32, f32[256]{0:T(256)S(1)} %add_rsqrt_fusion.3), kind=kOutput, calls=%fused_computation.29 | convolution fusion | flops 537395200 | bytes 3671040 | tf_op jit(solution)/shard_map/dot_general | solution.py:147
  37.7 5.8 %collective-permute-start = (bf16[15,512]{1,0:T(8,128)(2,1)S(1)}, bf16[15,512]{1,0:T(8,128)(2,1)S(1)}, u32[]{:S(2)}, u32[]{:S(2)}) collective-permute-start(bf16[15,512]{1,0:T(8,128)(2,1)S(1)} %get-tuple-element.158), channel_id=1, source_target_pairs={{0,4},{4,8},{8,12},{12,16},{16,20},{20,24},{24,28},{28,32},{32,36}... | collective-permute-start | bytes 46088 | tf_op jit(solution)/shard_map/ppermute | solution.py:45
  43.6 1.9 collective-permute-start.1
  47.0 1.6 collective-permute-done.1
  48.7 2.6 fusion.58
  51.9 3.2 %all-to-all-start.1 = ((f32[4,1,256]{2,1,0:T(1,128)}), f32[4,1,256]{2,1,0:T(1,128)S(1)}, u32[]{:S(2)}, u32[]{:S(2)}) async-start(f32[4,1,256]{2,1,0:T(1,128)} %broadcast_in_dim.18), calls=%async_computation.1 | async-start | bytes 8192 | tf_op jit(solution)/shard_map/all_to_all | solution.py:21
  55.2 4.2 %all-to-all-done.1 = f32[4,1,256]{2,1,0:T(1,128)S(1)} async-done(((f32[4,1,256]{2,1,0:T(1,128)}), f32[4,1,256]{2,1,0:T(1,128)S(1)}, u32[]{:S(2)}, u32[]{:S(2)}) %all-to-all-start.1) | async-done | bytes 4128 | tf_op jit(solution)/shard_map/all_to_all | solution.py:21
  60.2 3.2 %all-to-all-start.2 = ((f32[4,1,256]{2,1,0:T(1,128)}), f32[4,1,256]{2,1,0:T(1,128)S(1)}, u32[]{:S(2)}, u32[]{:S(2)}) async-start(f32[4,1,256]{2,1,0:T(1,128)} %broadcast_in_dim.19), calls=%async_computation.2 | async-start | bytes 8192 | tf_op jit(solution)/shard_map/all_to_all | solution.py:21
  63.5 4.1 %all-to-all-done.2 = f32[4,1,256]{2,1,0:T(1,128)S(1)} async-done(((f32[4,1,256]{2,1,0:T(1,128)}), f32[4,1,256]{2,1,0:T(1,128)S(1)}, u32[]{:S(2)}, u32[]{:S(2)}) %all-to-all-start.2) | async-done | bytes 4128 | tf_op jit(solution)/shard_map/all_to_all | solution.py:21
  67.6 76.5 %all-gather.2.cloned.1.call-done = bf16[16384,544]{0,1:T(8,128)(2,1)} async-done(((bf16[256,544]{0,1:T(8,128)(2,1)}), bf16[16384,544]{0,1:T(8,128)(2,1)}) %all-gather.2.cloned.1.call-update) | async-done | bytes 17825808 | tf_op jit(solution)/shard_map/all_gather | solution.py:34
  144.1 1.3 split.13
  146.5 6.7 %fusion.61 = (bf16[16384,256]{0,1:T(8,128)(2,1)S(1)}, bf16[16384,256]{0,1:T(8,128)(2,1)S(1)}) fusion(bf16[16384,544]{0,1:T(8,128)(2,1)} %all-gather.2.cloned.1.call-done), kind=kLoop, calls=%fused_computation.134 | loop fusion | bytes 33554432 | tf_op jit(solution)/shard_map/split | solution.py:34
  153.2 6.2 %copy_bitcast_fusion = (bf16[16,1024,256]{1,2,0:T(8,128)(2,1)}, bf16[16,1024,256]{1,2,0:T(8,128)(2,1)}) fusion(bf16[32,16,8,1024]{3,2,1,0:T(8,128)(2,1)S(1)} %bitcast.109, bf16[32,16,8,1024]{3,2,1,0:T(8,128)(2,1)S(1)} %bitcast.110), kind=kLoop, calls=%fused_computation.18 | loop fusion | bytes 33554432
  159.4 81.2 %while.15 = (s32[]{:T(128)}, f32[4,256]{1,0:T(4,128)S(1)}, f32[4,256]{1,0:T(4,128)S(1)}, f32[4,256,64]{1,2,0:T(8,128)S(1)}, bf16[16,1024,256]{1,2,0:T(8,128)(2,1...) while((s32[]{:T(128)}, f32[4,256]{1,0:T(4,128)S(1)}, ...), condition=%wide.region_6.7_spmd.clone, body=%wide.region_3.6_spmd.clone.sunk | while | flops 343086080 | bytes 24969352 | solution.py:115
  159.4 1.3 constant_dynamic-slice_fusion.3
  161.5 1.6 fusion.104
  164.5 1.3 constant_dynamic-slice_fusion.3
  166.6 1.6 fusion.104
  169.6 1.3 constant_dynamic-slice_fusion.3
  171.6 1.6 fusion.104
  174.7 1.3 constant_dynamic-slice_fusion.3
  176.7 1.6 fusion.104
  179.8 1.3 constant_dynamic-slice_fusion.3
  181.8 1.6 fusion.104
  184.8 1.3 constant_dynamic-slice_fusion.3
  186.9 1.6 fusion.104
  189.9 1.3 constant_dynamic-slice_fusion.3
  192.0 1.6 fusion.104
  195.0 1.3 constant_dynamic-slice_fusion.3
  197.0 1.6 fusion.104
  200.1 1.3 constant_dynamic-slice_fusion.3
  202.1 1.6 fusion.104
  205.1 1.3 constant_dynamic-slice_fusion.3
  207.2 1.6 fusion.104
  210.2 1.3 constant_dynamic-slice_fusion.3
  212.3 1.6 fusion.104
  215.3 1.3 constant_dynamic-slice_fusion.3
  217.3 1.6 fusion.104
  222.4 1.6 fusion.104
  227.5 1.6 fusion.104
  230.5 1.3 constant_dynamic-slice_fusion.3
  232.6 1.6 fusion.104
  235.6 1.3 constant_dynamic-slice_fusion.3
  237.7 1.6 fusion.104
  240.7 1.7 fusion.66
  243.4 18.4 %all_to_all.22 = bf16[4,512,256]{1,2,0:T(8,128)(2,1)S(1)} all-to-all(bf16[4,512,256]{1,2,0:T(8,128)(2,1)S(1)} %bitcast.112), channel_id=1, replica_groups=mesh['sp'=64,'tp'=4] {'tp'}, dimensions={0} | all-to-all | bytes 2097152 | tf_op jit(solution)/shard_map/all_to_all | solution.py:66
  (171 shorter events, 52.9 us)
Async XLA Ops:
  6.5 235.9 %copy-start = (bf16[512,2048]{1,0:T(8,128)(2,1)S(1)}, bf16[512,2048]{1,0:T(8,128)(2,1)}, u32[]{:S(2)}) copy-start(bf16[512,2048]{1,0:T(8,128)(2,1)} %param.37) | copy-start | bytes 6291460
  6.5 20.9 %copy-start.7 = (f32[2048]{0:T(1024)S(1)}, f32[2048]{0:T(1024)}, u32[]{:S(2)}) copy-start(f32[2048]{0:T(1024)} %param.21) | copy-start | bytes 24580
  6.5 21.3 %copy-start.6 = (bf16[2048,32]{0,1:T(8,128)(2,1)S(1)}, bf16[2048,32]{0,1:T(8,128)(2,1)}, u32[]{:S(2)}) copy-start(bf16[2048,32]{0,1:T(8,128)(2,1)} %param.24) | copy-start | bytes 393220
  8.8 20.6 %copy-start.4 = (bf16[256,256]{1,0:T(8,128)(2,1)S(1)}, bf16[256,256]{1,0:T(8,128)(2,1)}, u32[]{:S(2)}) copy-start(bf16[256,256]{1,0:T(8,128)(2,1)} %param.30) | copy-start | bytes 393220
  8.8 20.6 %copy-start.9 = (f32[256]{0:T(256)S(1)}, f32[256]{0:T(256)}, u32[]{:S(2)}) copy-start(f32[256]{0:T(256)} %param.26) | copy-start | bytes 3076
  8.8 18.3 %all-to-all-start = ((bf16[4,256,512]{1,2,0:T(8,128)(2,1)}), bf16[4,256,512]{1,2,0:T(8,128)(2,1)S(1)}, u32[]{:S(2)}, u32[]{:S(2)}) async-start(bf16[4,256,512]{1,2,0:T(8,128)(2,1)} %broadcast_in_dim.17), calls=%async_computation | async-start | bytes 2097152 | tf_op jit(solution)/shard_map/all_to_all | solution.py:21
  13.8 130.3 %all-gather.2.cloned.1.call-start = ((), (), s32[]{:S(2)}) async-start(), calls=%async_computation.4 | async-start | bytes 18104320 | tf_op jit(solution)/shard_map/all_gather | solution.py:34
  27.1 1.7 copy-start.13
  27.8 1.0 copy-start.1
  29.4 7.5 %copy-start.2 = (bf16[256,2048]{0,1:T(8,128)(2,1)S(1)}, bf16[256,2048]{0,1:T(8,128)(2,1)}, u32[]{:S(2)}) copy-start(bf16[256,2048]{0,1:T(8,128)(2,1)} %copy-done.1) | copy-start | bytes 3145732
  31.8 5.1 %copy-start.11 = (bf16[2048,512]{1,0:T(8,128)(2,1)S(1)}, bf16[2048,512]{1,0:T(8,128)(2,1)}, u32[]{:S(2)}) copy-start(bf16[2048,512]{1,0:T(8,128)(2,1)} %param.31) | copy-start | bytes 6291460
  34.0 11.4 %copy-start.12 = (bf16[2048,512]{1,0:T(8,128)(2,1)S(1)}, bf16[2048,512]{1,0:T(8,128)(2,1)}, u32[]{:S(2)}) copy-start(bf16[2048,512]{1,0:T(8,128)(2,1)} %param.22) | copy-start | bytes 6291460
  37.0 9.4 %copy-start.3 = (bf16[512,256]{1,0:T(8,128)(2,1)S(1)}, bf16[512,256]{1,0:T(8,128)(2,1)}, u32[]{:S(2)}) copy-start(bf16[512,256]{1,0:T(8,128)(2,1)} %param.27) | copy-start | bytes 786436
  37.0 9.4 %copy-start.8 = (f32[512]{0:T(512)S(1)}, f32[512]{0:T(512)}, u32[]{:S(2)}) copy-start(f32[512]{0:T(512)} %param.25) | copy-start | bytes 6148
  37.0 9.7 %copy-start.5 = (bf16[512,128]{1,0:T(8,128)(2,1)S(1)}, bf16[512,128]{1,0:T(8,128)(2,1)}, u32[]{:S(2)}) copy-start(bf16[512,128]{1,0:T(8,128)(2,1)} %param.28) | copy-start | bytes 393220
  37.7 11.0 %copy-start.10 = (f32[512]{0:T(512)S(1)}, f32[512]{0:T(512)}, u32[]{:S(2)}) copy-start(f32[512]{0:T(512)} %param.34) | copy-start | bytes 6148
  37.7 9.3 %collective-permute-start = (bf16[15,512]{1,0:T(8,128)(2,1)S(1)}, bf16[15,512]{1,0:T(8,128)(2,1)S(1)}, u32[]{:S(2)}, u32[]{:S(2)}) collective-permute-start(bf16[15,512]{1,0:T(8,128)(2,1)S(1)} %get-tuple-element.158), channel_id=1, source_target_pairs={{0,4},{4,8},{8,12},{12,16},{16,20},{20,24},{24,28},{28,32},{32,36}... | collective-permute-start | bytes 46088 | tf_op jit(solution)/shard_map/ppermute | solution.py:45
  43.6 5.1 %collective-permute-start.1 = (bf16[15,512]{1,0:T(8,128)(2,1)S(1)}, bf16[15,512]{1,0:T(8,128)(2,1)S(1)}, u32[]{:S(2)}, u32[]{:S(2)}) collective-permute-start(bf16[15,512]{1,0:T(8,128)(2,1)S(1)} %get-tuple-element.159), channel_id=1, source_target_pairs={{4,0},{8,4},{12,8},{16,12},{20,16},{24,20},{28,24},{32,28},{36,32}... | collective-permute-start | bytes 46088 | tf_op jit(solution)/shard_map/ppermute | solution.py:47
  51.9 7.5 %all-to-all-start.1 = ((f32[4,1,256]{2,1,0:T(1,128)}), f32[4,1,256]{2,1,0:T(1,128)S(1)}, u32[]{:S(2)}, u32[]{:S(2)}) async-start(f32[4,1,256]{2,1,0:T(1,128)} %broadcast_in_dim.18), calls=%async_computation.1 | async-start | bytes 8192 | tf_op jit(solution)/shard_map/all_to_all | solution.py:21
  60.2 7.4 %all-to-all-start.2 = ((f32[4,1,256]{2,1,0:T(1,128)}), f32[4,1,256]{2,1,0:T(1,128)S(1)}, u32[]{:S(2)}, u32[]{:S(2)}) async-start(f32[4,1,256]{2,1,0:T(1,128)} %broadcast_in_dim.19), calls=%async_computation.2 | async-start | bytes 8192 | tf_op jit(solution)/shard_map/all_to_all | solution.py:21
  159.4 83.0 %copy-start.14 = (f32[512]{0:T(512)S(1)}, f32[512]{0:T(512)}, u32[]{:S(2)}) copy-start(f32[512]{0:T(512)} %param.35) | copy-start | bytes 6148
Sparse Core Ops, SparseCore 0:
  31.9 112.1 all-gather.1
where the time goes:
time: 271 us; the launch traced here: 270 us
  waiting for transfers between devices  99.7 us (37%)
  matrix products  60.4 us (22%)
  local copies, waits for them, and re-layouts  42.3 us (16%)
  starting transfers between devices  19.2 us (7%)
  blocking collectives  18.4 us (7%)
  other arithmetic  14.9 us (5%)
  between operations  13.8 us (5%)
    all_gather x1, waiting for transfers between devices, sent_together(): lax.all_gather(both, axis, axis=dim, tiled=True)  76.5 us
    dot_general x16, matrix products, attend_block(): jnp.einsum('qhd,kd->hqk', r_heads, rope_key, preferred_element_type=jnp.f...  25.5 us
    all_to_all x3, waiting for transfers between devices, sent_to_all(): return lax.all_to_all(copies, axis, split_axis=0, concat_axis=0, tiled=True)  21.6 us
    dynamic_slice x16, local copies, waits for them, and re-layouts, over_blocks(): state, unused = lax.scan(one_block, state, shaped)  20.4 us
    all_to_all x1, blocking collectives, sum_at_owner(): lax.all_to_all(blocks, axis, split_axis=0, concat_axis=0, tiled=True)  18.4 us
    dot_general x16, matrix products, attend_block(): jnp.einsum('hqk,khd->hqd', weight.astype(jnp.bfloat16), value_heads, pref...  12.8 us
    dot_general x16, matrix products, attend_block(): jnp.einsum('qhd,khd->hqk', q_heads, key_heads, preferred_element_type=jnp...  12.2 us
    all_to_all x3, starting transfers between devices, sent_to_all(): return lax.all_to_all(copies, axis, split_axis=0, concat_axis=0, tiled=True)  11.5 us
  transfers between devices with their start and end apart: 6, of which 5 were waited for; matrix products, arithmetic and copies ran while one was open for 4% of the time, Pallas kernels for 0%

commit v1 on v0

v1 whole, which is shorter than its diff:
```python
import functools
import math

import jax
import jax.numpy as jnp
from jax import lax
from jax.experimental import pallas as pl
from jax.experimental.pallas import tpu as pltpu
from jax.sharding import PartitionSpec as P


eps_norm = 1e-06
eps_layer = 1e-05
theta = 10000.0
Z, Y, C = 8, 4, 2
f32 = jnp.float32
bf16 = jnp.bfloat16
LANES = 128
EXTRA = 16


def moved(values, dz=0, dy=0, dc=0):
    pairs = []
    for z in range(Z):
        for y in range(Y):
            for c in range(C):
                to = (((z + dz) % Z) * Y + (y + dy) % Y) * C + (c + dc) % C
                pairs.append(((z * Y + y) * C + c, to))
    return lax.ppermute(values, "sp", pairs)


def passed_on(values):
    pairs = []
    for z in range(Z):
        for y in range(Y):
            for c in range(C):
                pairs.append(((z * Y + y) * C + c, (((z + 1 - 2 * c) % Z) * Y + y) * C + c))
    return lax.ppermute(values, "sp", pairs)


def moved_tp(values, step):
    count = lax.axis_size("tp")
    return lax.ppermute(values, "tp", [(i, (i + step) % count) for i in range(count)])


def in_order(me, came):
    ordered = []
    for j in range(4):
        k = lax.rem(j - me + 4, 4)
        ordered.append(
            jnp.where(k == 0, came[0], jnp.where(k == 1, came[1], jnp.where(k == 2, came[2], came[3])))
        )
    return ordered


def prepare_kernel(heads, key_up, value_up, kup, vup, place):
    nope = key_up.shape[1] // heads
    gap = jnp.zeros((key_up.shape[0], LANES - nope), bf16)
    for h in range(heads):
        kup[:, h * LANES : (h + 1) * LANES] = jnp.concatenate(
            [key_up[:, h * nope : (h + 1) * nope], gap], axis=1
        )
    vup[...] = jnp.transpose(value_up[...])
    row = lax.broadcasted_iota(jnp.int32, place.shape, 0)
    column = lax.broadcasted_iota(jnp.int32, place.shape, 1)
    place[...] = jnp.where(column == row + nope, 1.0, 0.0).astype(bf16)


def prepare(key_up, value_up, heads, rope_size):
    vmem = pl.BlockSpec(memory_space=pltpu.VMEM)
    return pl.pallas_call(
        functools.partial(prepare_kernel, heads),
        out_shape=(
            jax.ShapeDtypeStruct((key_up.shape[0], heads * LANES), bf16),
            jax.ShapeDtypeStruct(value_up.shape[::-1], bf16),
            jax.ShapeDtypeStruct((rope_size, LANES), bf16),
        ),
        in_specs=[vmem] * 2,
        out_specs=(vmem,) * 3,
        cost_estimate=pl.CostEstimate(flops=10**7, bytes_accessed=10**6, transcendentals=0),
        compiler_params=pltpu.CompilerParams(vmem_limit_bytes=8 * 2**20),
        name="prepare",
    )(key_up, value_up)


def attend_kernel(sizes, nq, heads, first, last, scale, skip, *refs):
    nl = len(sizes)
    lat = [refs[k].at[j] for k, size in enumerate(sizes) for j in range(size)]
    kup, vup, place = refs[nl : nl + 3]
    q = refs[nl + 3 : nl + 3 + nq]
    at = nl + 3 + nq
    if not first:
        state, high = refs[at : at + 2]
        at += 2
    if last:
        out = refs[at]
        at += 1
    else:
        out, out_high = refs[at : at + 2]
        at += 2
    kbuf, vbuf, qbuf, sa, sb, pa, pb, ma, mb, tops = refs[at:]
    keys = lat[0].shape[1]
    rank = kup.shape[0]
    vdim = vup.shape[0] // heads
    n = len(lat) * keys
    items = nq * heads
    dq = q[0].shape[0] // heads
    for b, ref in enumerate(lat):
        block = ref[:rank]
        rope = lax.dot_general(
            ref[rank:], place[...], (((0,), (0,)), ((), ())), preferred_element_type=f32
        )
        kk = jnp.dot(block, kup[...], preferred_element_type=f32)
        vv = lax.dot_general(vup[...], block, (((1,), (1,)), ((), ())), preferred_element_type=f32)
        rows = slice(b * keys, (b + 1) * keys)
        for h in range(heads):
            kbuf[h, rows, :] = (kk[:, h * LANES : (h + 1) * LANES] + rope).astype(bf16)
            vbuf[h, :vdim, rows] = vv[h * vdim : (h + 1) * vdim].astype(bf16)
    for h in range(heads):
        vbuf[h, vdim:, :] = jnp.ones((vbuf.shape[1] - vdim, n), bf16)
    for i in range(nq):
        for h in range(heads):
            qbuf[i * heads + h, :dq, :] = q[i][h * dq : (h + 1) * dq]
            qbuf[i * heads + h, dq:, :] = jnp.zeros((LANES - dq, q[i].shape[1]), bf16)

    def scores(i, s_ref, m_ref):
        s = jnp.dot(kbuf[lax.rem(i, heads)], qbuf[i], preferred_element_type=f32) * scale
        s_ref[...] = s
        top = jnp.max(s, axis=0, keepdims=True)
        if not first:
            before = high[i + skip][:1]
            top = jnp.maximum(top, before)
        top = top.astype(bf16).astype(f32)
        shrink = top if first else jnp.exp2(before - top)
        m_ref[...] = jnp.broadcast_to(top, m_ref.shape)
        tops[i] = jnp.concatenate([jnp.broadcast_to(v, (8, v.shape[1])) for v in (top, shrink)])

    def weights(s_ref, m_ref, p_ref):
        p_ref[...] = jnp.exp2(s_ref[...] - m_ref[:1]).astype(bf16)

    def values(i, p_ref):
        o = jnp.dot(vbuf[lax.rem(i, heads)], p_ref[...], preferred_element_type=f32)
        top = tops[i, :8]
        if not first:
            o = o + state[i + skip] * tops[i, 8:9]
        if not last:
            out[i] = o
            out_high[i] = top
            return
        total = o[vdim : vdim + 8]
        total_high = total.astype(bf16).astype(f32)
        row = lax.broadcasted_iota(jnp.int32, total.shape, 0)
        tail = jnp.where(row == 0, total_high, jnp.where(row == 1, total - total_high, top))
        out[i] = jnp.concatenate([o[:vdim], tail, tail], axis=0).astype(bf16)

    scores(0, sa, ma)
    scores(1, sb, mb)
    weights(sa, ma, pa)

    def step(j, carry):
        i = 2 * j
        scores(i + 2, sa, ma)
        weights(sb, mb, pb)
        values(i, pa)
        scores(i + 3, sb, mb)
        weights(sa, ma, pa)
        values(i + 1, pb)
        return carry

    lax.fori_loop(0, items // 2 - 1, step, 0)
    weights(sb, mb, pb)
    values(items - 2, pa)
    values(items - 1, pb)


def attend(lat, kup, vup, place, q, heads, scale, state=None, last=False, skip=0):
    nq = len(q)
    sizes = [item.shape[0] for item in lat]
    keys, toks = lat[0].shape[2], q[0].shape[1]
    n = sum(sizes) * keys
    rows = vup.shape[0] // heads + EXTRA
    items = nq * heads
    first = state is None
    args = [*lat, kup, vup, place, *q] + ([] if first else list(state))
    vmem = pl.BlockSpec(memory_space=pltpu.VMEM)
    if last:
        out_shape = (jax.ShapeDtypeStruct((items, rows, toks), bf16),)
    else:
        out_shape = (
            jax.ShapeDtypeStruct((items, rows, toks), f32),
            jax.ShapeDtypeStruct((items, 8, toks), f32),
        )
    return pl.pallas_call(
        functools.partial(attend_kernel, sizes, nq, heads, first, last, scale, skip),
        out_shape=out_shape,
        in_specs=[vmem] * len(args),
        out_specs=(vmem,) * len(out_shape),
        scratch_shapes=[
            pltpu.VMEM((heads, n, LANES), bf16),
            pltpu.VMEM((heads, rows, n), bf16),
            pltpu.VMEM((items, LANES, toks), bf16),
            pltpu.VMEM((n, toks), f32),
            pltpu.VMEM((n, toks), f32),
            pltpu.VMEM((n, toks), bf16),
            pltpu.VMEM((n, toks), bf16),
            pltpu.VMEM((8, toks), f32),
            pltpu.VMEM((8, toks), f32),
            pltpu.VMEM((items, 16, toks), f32),
        ],
        cost_estimate=pl.CostEstimate(
            flops=2 * items * toks * n * 336, bytes_accessed=4 * 2**20, transcendentals=items * toks * n
        ),
        compiler_params=pltpu.CompilerParams(vmem_limit_bytes=24 * 2**20),
        name="attend",
    )(*args)


def merge_kernel(heads, me, *refs):
    parts = refs[:4]
    w_ref, conv_ref = refs[4:6]
    outs = refs[6:10]
    rows, toks = parts[0].shape[1:]
    vdim = rows - EXTRA
    columns = []
    for h in range(heads):
        tops = [p[h, vdim + 2 : vdim + 3].astype(f32) for p in parts]
        top = functools.reduce(jnp.maximum, tops)
        total = jnp.zeros((1, toks), f32)
        sums = jnp.zeros((vdim, toks), f32)
        for p, t in zip(parts, tops):
            factor = jnp.exp2(t - top)
            ends = p[h, vdim : vdim + 2].astype(f32)
            total = total + (ends[:1] + ends[1:]) * factor
            sums = sums + p[h, :vdim].astype(f32) * factor
        columns.append((sums / total).astype(bf16))
    attended = jnp.concatenate(columns, axis=0)
    feats = outs[0].shape[1]
    for k in range(4):
        at = pl.multiple_of(lax.rem(me[0] + k, 4) * feats, feats)
        part = lax.dot_general(
            attended, w_ref[:, pl.ds(at, feats)], (((0,), (0,)), ((), ())), preferred_element_type=f32
        )
        outs[k][...] = (part + conv_ref[:, pl.ds(at, feats)]).astype(bf16)


def merge(me, parts, out_attend, conv_part):
    heads, _, toks = parts[0].shape
    vmem = pl.BlockSpec(memory_space=pltpu.VMEM)
    shape = jax.ShapeDtypeStruct((toks, out_attend.shape[1] // 4), bf16)
    return pl.pallas_call(
        functools.partial(merge_kernel, heads),
        out_shape=(shape,) * 4,
        in_specs=[pl.BlockSpec(memory_space=pltpu.SMEM)] + [vmem] * 6,
        out_specs=(vmem,) * 4,
        cost_estimate=pl.CostEstimate(
            flops=2 * toks * out_attend.size, bytes_accessed=5 * 2**20, transcendentals=0
        ),
        compiler_params=pltpu.CompilerParams(vmem_limit_bytes=16 * 2**20),
        name="merge",
    )(jnp.reshape(me, (1,)).astype(jnp.int32), *parts, out_attend, conv_part)


def rms_scale(values, gain):
    return values * lax.rsqrt(jnp.mean(values * values, axis=-1, keepdims=True) + eps_norm) * gain


def rotate_rows(values, positions):
    half = values.shape[-2] // 2
    freqs = theta ** (-jnp.arange(half).astype(f32) / half)
    angles = freqs[:, None] * positions
    cosine = jnp.cos(angles)
    sine = jnp.sin(angles)
    first = values[..., :half, :]
    second = values[..., half:, :]
    return jnp.concatenate(
        [first * cosine - second * sine, second * cosine + first * sine], axis=-2
    )


def columns(weight, rows):
    return lax.dot_general(weight, rows, (((0,), (1,)), ((), ())), preferred_element_type=f32)


def per_device(
    tokens,
    in_gain,
    query_down,
    latent_down,
    rope_down,
    query_gain,
    latent_gain,
    query_nope,
    query_rope,
    key_up,
    value_up,
    conv_value,
    conv_gate,
    conv_taps,
    conv_bias,
    channel_gain,
    out_attend,
    out_conv,
):
    row_count = tokens.shape[0]
    width = in_gain.shape[0]
    local_ch = conv_value.shape[1]
    sp = lax.axis_index("sp")
    positions = (sp * row_count + jnp.arange(row_count)).astype(f32)
    rope_size = rope_down.shape[1]
    heads = query_rope.shape[1] // rope_size
    nope = key_up.shape[1] // heads
    score_scale = (nope + rope_size) ** -0.5 * math.log2(math.e)

    me = lax.axis_index("tp")
    came = [tokens] + [moved_tp(tokens, step) for step in (-1, 2, 1)]
    piece_f = jnp.concatenate(in_order(me, came), axis=1).astype(f32)
    scaled = (piece_f * in_gain).astype(bf16)
    square_sum = jnp.sum(piece_f * piece_f, axis=1)
    row_scale = lax.rsqrt(square_sum / width + eps_norm)[:, None]

    def add_rows(weight):
        return jnp.dot(scaled, weight, preferred_element_type=f32)

    kv_latent = rms_scale(row_scale * add_rows(latent_down), latent_gain).astype(bf16)
    rope_key = rotate_rows(columns(rope_down, scaled) * row_scale[:, 0], positions).astype(bf16)
    lat = jnp.concatenate([kv_latent, rope_key], axis=0)
    q_latent = rms_scale(row_scale * add_rows(query_down), query_gain).astype(bf16)
    q_flat = columns(query_nope, q_latent).astype(bf16).reshape(heads, nope, row_count)
    q_turn = columns(query_rope, q_latent).reshape(heads, rope_size, row_count)
    r_flat = rotate_rows(q_turn, positions).astype(bf16)
    q_own = jnp.concatenate([q_flat, r_flat], axis=1).reshape(heads * (nope + rope_size), row_count)

    q_far = [moved(q_own, dy=d) for d in (1, -1, 2)]

    own = jnp.stack([lat, moved(lat, dc=1)])
    hop1 = passed_on(own)
    hop2 = passed_on(hop1)
    hop3 = passed_on(hop2)
    hop4 = passed_on(hop3[:1])
    side1, side2, side3, side4 = (
        moved(hop, dc=1) for hop in (hop1, hop2, hop3, hop4)
    )

    kup, vup, place = prepare(key_up, value_up, heads, rope_size)

    def part(blocks, queries, state=None, last=False, skip=0):
        return attend(
            blocks, kup, vup, place, queries, heads, score_scale, state, last, skip
        )

    glu = (
        row_scale * add_rows(conv_value) * jax.nn.sigmoid(row_scale * add_rows(conv_gate))
    ).astype(bf16)
    taps = conv_taps.shape[0]
    reach = taps // 2
    count = lax.axis_size("sp")
    before = lax.ppermute(glu[row_count - reach :], "sp", [(i, i + 1) for i in range(count - 1)])
    after = lax.ppermute(glu[:reach], "sp", [(i + 1, i) for i in range(count - 1)])
    padded = jnp.concatenate([before, glu, after], axis=0).astype(f32)
    conv = jnp.zeros((row_count, local_ch), f32) + conv_bias
    for tap in range(taps):
        conv = conv + conv_taps[tap] * padded[tap : tap + row_count]
    own_mean = jnp.mean(conv, axis=-1)
    own_off = conv - own_mean[:, None]
    own_stats = jnp.stack([own_mean, jnp.sum(own_off * own_off, axis=-1)])
    stats = jnp.stack([own_stats] + [moved_tp(own_stats, k) for k in (1, -1, 2)])
    mean = jnp.mean(stats[:, 0], axis=0)
    apart = stats[:, 0] - mean
    spread = jnp.sum(stats[:, 1] + local_ch * apart * apart, axis=0) / (4 * local_ch)
    activated = jax.nn.silu(
        (conv - mean[:, None]) * lax.rsqrt(spread + eps_layer)[:, None] * channel_gain
    ).astype(bf16)

    conv_part = jnp.dot(activated, out_conv, preferred_element_type=f32)

    own_first = [q_own] + q_far
    state = part([own, hop1], own_first)
    state = part([side1, hop2], own_first, state)
    state = part([side2, hop3], own_first, state)
    ends = [side3, hop4, side4]
    (packed,) = part(ends, q_far, state, True, heads)
    packed = packed.reshape((3, heads) + packed.shape[1:])

    parts = [moved(packed[k], dy=d) for k, d in enumerate((-1, 1, 2))]
    (packed_own,) = part(ends, [q_own], state, True)
    cuts = merge(me, [packed_own] + parts, out_attend, conv_part)
    mixed = cuts[0].astype(f32)
    for k, step in ((1, 1), (2, 2), (3, -1)):
        mixed = mixed + moved_tp(cuts[k], step).astype(f32)
    return mixed.astype(bf16)


def solution(mesh):
    in_specs = (
        P("sp", "tp"),
        P(),
        P(),
        P(),
        P(),
        P(),
        P(),
        P(None, "tp"),
        P(None, "tp"),
        P(None, "tp"),
        P(None, "tp"),
        P(None, "tp"),
        P(None, "tp"),
        P(None, "tp"),
        P("tp"),
        P("tp"),
        P("tp", None),
        P("tp", None),
    )
    out_specs = P("sp", "tp")


    return jax.shard_map(
        per_device, mesh=mesh, in_specs=in_specs, out_specs=out_specs, check_vma=False
    )
```

time: 271 us -> 116 us (0.43)
  waiting for transfers between devices: 99.7 us -> 27.9 us
  matrix products: 60.4 us -> 4.79 us
  local copies, waits for them, and re-layouts: 42.3 us -> 5.65 us
  Pallas kernels: 0 us -> 26.5 us
  starting transfers between devices: 19.2 us -> 44.5 us
  blocking collectives: 18.4 us -> 0 us
  between operations: 13.8 us -> 0.48 us
  other arithmetic: 14.9 us -> 5.51 us
    all_gather x1 -> x0, waiting for transfers between devices: 76.5 us -> none  [sent_together(): lax.all_gather(both, axis, axis=dim, tiled=True)]
    dot_general x59 -> x8, matrix products: 60.4 us -> 4.79 us  [the longest x4 2.88 us: add_rows(): return jnp.dot(scaled, weight, preferred_element_type=f32)]
    ppermute x2 -> x26, starting transfers between devices: 7.73 us -> 44.5 us  [the longest x4 14.5 us: passed_on(): return lax.ppermute(values, 'sp', pairs)]
    pallas_call x0 -> x7, Pallas kernels: none -> 26.5 us  [the longest x5 25.8 us: attend(): pl.pallas_call(functools.partial(attend_kernel, sizes, nq, heads, first,...]
    ppermute x2 -> x26, waiting for transfers between devices: 1.61 us -> 27.9 us  [the longest x9 17.3 us: moved_tp(): lax.ppermute(values, 'tp', [(i, (i + step) % count) for i in range(count)])]
    all_to_all x3 -> x0, waiting for transfers between devices: 21.6 us -> none  [sent_to_all(): return lax.all_to_all(copies, axis, split_axis=0, concat_axis=0, tiled=True)]
    dynamic_slice x16 -> x0, local copies, waits for them, and re-layouts: 20.4 us -> none  [over_blocks(): state, unused = lax.scan(one_block, state, shaped)]
    all_to_all x1 -> x0, blocking collectives: 18.4 us -> none  [sum_at_owner(): lax.all_to_all(blocks, axis, split_axis=0, concat_axis=0, tiled=True)]
  transfers between devices with their start and end apart: 6 -> 26, of which waited for: 5 -> 9; matrix products, arithmetic and copies ran while one was open for 4% -> 8% of each run, Pallas kernels for 0% -> 18%
where the time goes in v1:
time: 116 us; the launch traced here: 115 us
  starting transfers between devices  44.5 us (38%)
  waiting for transfers between devices  27.9 us (24%)
  Pallas kernels  26.5 us (23%)
  local copies, waits for them, and re-layouts  5.65 us (5%)
  other arithmetic  5.51 us (5%)
  matrix products  4.79 us (4%)
    pallas_call x5, Pallas kernels, attend(): pl.pallas_call(functools.partial(attend_kernel, sizes, nq, heads, first,...  25.8 us
    ppermute x9, waiting for transfers between devices, moved_tp(): lax.ppermute(values, 'tp', [(i, (i + step) % count) for i in range(count)])  17.3 us
    ppermute x4, starting transfers between devices, passed_on(): return lax.ppermute(values, 'sp', pairs)  14.5 us
    ppermute x9, starting transfers between devices, moved_tp(): lax.ppermute(values, 'tp', [(i, (i + step) % count) for i in range(count)])  13.3 us
    ppermute x11, starting transfers between devices, moved(): return lax.ppermute(values, 'sp', pairs)  11 us
    ppermute x11, waiting for transfers between devices, moved(): return lax.ppermute(values, 'sp', pairs)  4.71 us
    ppermute x1, starting transfers between devices, per_device(): lax.ppermute(glu[row_count - reach:], 'sp', [(i, i + 1) for i in range(co...  3.83 us
    ppermute x4, waiting for transfers between devices, passed_on(): return lax.ppermute(values, 'sp', pairs)  3.56 us
  transfers between devices with their start and end apart: 26, of which 9 were waited for; matrix products, arithmetic and copies ran while one was open for 8% of the time, Pallas kernels for 18%

profile of v1, /device:TPU:1, one launch (start us, length us, event | category | flops | bytes accessed | tf_op | source)
XLA Modules:
  0.0 115.4 jit_solution(17187302276380716437)
XLA Ops:
  0.0 3.6 %collective-permute-start.1 = (bf16[256,512]{1,0:T(8,128)(2,1)}, bf16[256,512]{1,0:T(8,128)(2,1)S(1)}, u32[]{:S(2)}, u32[]{:S(2)}) collective-permute-start(bf16[256,512]{1,0:T(8,128)(2,1)} %param.18), channel_id=1, source_target_pairs={{0,2},{1,3},{2,0},{3,1},{4,6},{5,7},{6,4},{7,5},{8,10},{9,11},{10,... | collective-permute-start | bytes 786440 | tf_op jit(solution)/shard_map/ppermute | solution.py:43
  3.7 0.9 collective-permute-start
  4.5 0.6 collective-permute-start.2
  5.1 1.0 fusion.61
  6.2 0.9 copy-done.2
  7.1 0.9 copy-done.3
  8.1 1.2 %fusion.60 = (f32[1,512]{1,0:T(1,128)S(1)}, f32[1,512]{1,0:T(1,128)S(1)}, f32[1,512]{1,0:T(1,128)S(1)}, f32[1,512]{1,0:T(1,128)S(1)}, f32[1,512]{1,0:T(1,128)S(1...) fusion(f32[31,512]{1,0:T(8,128)} %param.31), kind=kLoop, calls=%fused_computation.129 | loop fusion | bytes 77824 | tf_op jit(solution)/shard_map/slice | solution.py:362
  9.3 6.3 %collective-permute-done = bf16[256,512]{1,0:T(8,128)(2,1)S(1)} collective-permute-done((bf16[256,512]{1,0:T(8,128)(2,1)}, bf16[256,512]{1,0:T(8,128)(2,1)S(1)}, u32[]{:S(2)}, u32[]{:S(2)}) %collective-permute-start) | collective-permute-done | bytes 262176 | tf_op jit(solution)/shard_map/ppermute | solution.py:43
  15.9 1.1 select_select_fusion.3
  17.8 0.8 copy-done.12
  19.4 1.3 %collective-permute-start.3 = (bf16[288,256]{1,0:T(8,128)(2,1)S(1)}, bf16[288,256]{1,0:T(8,128)(2,1)S(1)}, u32[]{:S(2)}, u32[]{:S(2)}) collective-permute-start(bf16[288,256]{1,0:T(8,128)(2,1)S(1)} %get-tuple-element.45), channel_id=1, source_target_pairs={{0,4},{4,0},{8,12},{12,8},{16,20},{20,16},{24,28},{28,24},{32,36},... | collective-permute-start | bytes 442376 | tf_op jit(solution)/shard_map/ppermute | solution.py:29
  20.8 0.8 fusion.5
  21.6 0.8 multiply_reduce_fusion.1
  22.4 0.8 copy-done.11
  23.2 0.7 fusion.7
  24.0 3.8 %collective-permute-start.18 = (bf16[15,512]{1,0:T(8,128)(2,1)S(1)}, bf16[15,512]{1,0:T(8,128)(2,1)S(1)}, u32[]{:S(2)}, u32[]{:S(2)}) collective-permute-start(bf16[15,512]{1,0:T(8,128)(2,1)S(1)} %get-tuple-element.40), channel_id=1, source_target_pairs={{0,4},{4,8},{8,12},{12,16},{16,20},{20,24},{24,28},{28,32},{32,36}... | collective-permute-start | bytes 46088 | tf_op jit(solution)/shard_map/ppermute | solution.py:357
  27.8 1.9 %collective-permute-start.19 = (bf16[15,512]{1,0:T(8,128)(2,1)S(1)}, bf16[15,512]{1,0:T(8,128)(2,1)S(1)}, u32[]{:S(2)}, u32[]{:S(2)}) collective-permute-start(bf16[15,512]{1,0:T(8,128)(2,1)S(1)} %get-tuple-element.41), channel_id=1, source_target_pairs={{4,0},{8,4},{12,8},{16,12},{20,16},{24,20},{28,24},{32,28},{36,32}... | collective-permute-start | bytes 46088 | tf_op jit(solution)/shard_map/ppermute | solution.py:358
  30.5 2.4 %collective-permute-done.19 = bf16[15,512]{1,0:T(8,128)(2,1)S(1)} collective-permute-done((bf16[15,512]{1,0:T(8,128)(2,1)S(1)}, bf16[15,512]{1,0:T(8,128)(2,1)S(1)}, u32[]{:S(2)}, u32[]{:S(2)}) %collective-permute-start.19) | collective-permute-done | bytes 15392 | tf_op jit(solution)/shard_map/ppermute | solution.py:358
  33.0 2.6 %fusion.56 = (f32[256]{0:T(256)S(1)}, f32[256,512]{1,0:T(8,128)S(1)}) fusion(f32[286,512]{1,0:T(8,128)S(1)} %maximum_convert_fusion, f32[512]{0:T(512)S(1)} %bitcast.87, f32[512]{0:T(512)S(1)} %bitcast.88, f32[512]{0:T(512)S(1)} %bitcast.90, f32[512]{0:T(512)S(1)} %bitcast.91, f32[512]{0:T(512)S(1)} %bitcast.92, f32[512]{0:T(512)S(1)} %bitcast.93, ...), kind=kLoop, calls=%fused_computation.126 | loop fusion | flops 8257280 | bytes 16843776 | tf_op jit(solution)/shard_map/reduce_sum | solution.py:363
  35.8 2.4 %collective-permute-start.21 = (f32[2,256]{1,0:T(2,128)S(1)}, f32[2,256]{1,0:T(2,128)S(1)}, u32[]{:S(2)}, u32[]{:S(2)}) collective-permute-start(f32[2,256]{1,0:T(2,128)S(1)} %get-tuple-element.80), channel_id=1, source_target_pairs={{0,3},{1,0},{2,1},{3,2},{4,7},{5,4},{6,5},{7,6},{8,11},{9,8},{10,9... | collective-permute-start | bytes 6152 | tf_op jit(solution)/shard_map/ppermute | solution.py:43
  38.2 1.7 %collective-permute-start.22 = (f32[2,256]{1,0:T(2,128)S(1)}, f32[2,256]{1,0:T(2,128)S(1)}, u32[]{:S(2)}, u32[]{:S(2)}) collective-permute-start(f32[2,256]{1,0:T(2,128)S(1)} %get-tuple-element.80), channel_id=1, source_target_pairs={{0,2},{1,3},{2,0},{3,1},{4,6},{5,7},{6,4},{7,5},{8,10},{9,11},{10,... | collective-permute-start | bytes 6152 | tf_op jit(solution)/shard_map/ppermute | solution.py:43
  39.9 5.7 %collective-permute-start.4 = (bf16[2,288,256]{2,1,0:T(8,128)(2,1)S(1)}, bf16[2,288,256]{2,1,0:T(8,128)(2,1)S(1)}, u32[]{:S(2)}, u32[]{:S(2)}) collective-permute-start(bf16[2,288,256]{2,1,0:T(8,128)(2,1)S(1)} %pad_maximum_fusion.1.refs_0_), channel_id=1, source_target_pairs={{0,32},{4,228},{8,40},{12,236},{16,48},{20,244},{24,56},{28,252},{... | collective-permute-start | bytes 884744 | tf_op jit(solution)/shard_map/ppermute | solution.py:38
  45.6 2.7 %collective-permute-start.13 = (bf16[384,256]{1,0:T(8,128)(2,1)S(1)}, bf16[384,256]{1,0:T(8,128)(2,1)S(1)}, u32[]{:S(2)}, u32[]{:S(2)}) collective-permute-start(bf16[384,256]{1,0:T(8,128)(2,1)S(1)} %bitcast.66), channel_id=1, source_target_pairs={{0,16},{4,20},{8,24},{12,28},{16,0},{20,4},{24,8},{28,12},{32,48},... | collective-permute-start | bytes 589832 | tf_op jit(solution)/shard_map/ppermute | solution.py:29
  48.3 1.1 collective-permute-start.12
  49.9 2.8 %collective-permute-start.5 = (bf16[2,288,256]{2,1,0:T(8,128)(2,1)S(1)}, bf16[2,288,256]{2,1,0:T(8,128)(2,1)S(1)}, u32[]{:S(2)}, u32[]{:S(2)}) collective-permute-start(bf16[2,288,256]{2,1,0:T(8,128)(2,1)S(1)} %collective-permute-done.4.refs_1_), channel_id=1, source_target_pairs={{0,32},{4,228},{8,40},{12,236},{16,48},{20,244},{24,56},{28,252},{... | collective-permute-start | bytes 884744 | tf_op jit(solution)/shard_map/ppermute | solution.py:38
  52.8 3.5 %collective-permute-done.5.refs_1_ = bf16[2,288,256]{2,1,0:T(8,128)(2,1)S(1)} collective-permute-done((bf16[2,288,256]{2,1,0:T(8,128)(2,1)S(1)}, bf16[2,288,256]{2,1,0:T(8,128)(2,1)S(1)}, u32[]{:S(2)}, u32[]{:S(2)}) %collective-permute-start.5) | collective-permute-done | bytes 294944 | tf_op jit(solution)/shard_map/ppermute | solution.py:38
  56.3 3.1 %collective-permute-start.6 = (bf16[2,288,256]{2,1,0:T(8,128)(2,1)S(1)}, bf16[2,288,256]{2,1,0:T(8,128)(2,1)S(1)}, u32[]{:S(2)}, u32[]{:S(2)}) collective-permute-start(bf16[2,288,256]{2,1,0:T(8,128)(2,1)S(1)} %collective-permute-done.5.refs_1_), channel_id=1, source_target_pairs={{0,32},{4,228},{8,40},{12,236},{16,48},{20,244},{24,56},{28,252},{... | collective-permute-start | bytes 884744 | tf_op jit(solution)/shard_map/ppermute | solution.py:38
  59.5 1.0 collective-permute-start.10
  60.4 6.2 %attend.5 = (f32[16,80,256]{2,1,0:T(8,128)S(1)}, f32[16,8,256]{2,1,0:T(8,128)S(1)}) custom-call(bf16[2,288,256]{2,1,0:T(8,128)(2,1)S(1)} %pad_maximum_fusion.1.refs_0_, bf16[2,288,256]{2,1,0:T(8,128)(2,1)S(1)} %collective-permute-done.4.refs_1_, bf16[256,512]{1,0:T(8,128)(2,1)S(1)} %get-tuple-element.18.refs_2_.refs_3_, ...), custom_call_target="tpu_custom_call" | custom-call | flops 2818572288 | bytes 4194304 | tf_op jit(solution)/shard_map/attend/pallas_call | solution.py:193
  66.6 2.9 %collective-permute-start.8 = (bf16[1,288,256]{2,1,0:T(8,128)(2,1)S(1)}, bf16[1,288,256]{2,1,0:T(8,128)(2,1)S(1)}, u32[]{:S(2)}, u32[]{:S(2)}) collective-permute-start(bf16[1,288,256]{2,1,0:T(8,128)(2,1)S(1)} %slice.302), channel_id=1, source_target_pairs={{0,32},{4,228},{8,40},{12,236},{16,48},{20,244},{24,56},{28,252},{... | collective-permute-start | bytes 442376 | tf_op jit(solution)/shard_map/ppermute | solution.py:38
  69.6 6.3 %attend.6 = (f32[16,80,256]{2,1,0:T(8,128)S(1)}, f32[16,8,256]{2,1,0:T(8,128)S(1)}) custom-call(bf16[2,288,256]{2,1,0:T(8,128)(2,1)S(1)} %collective-permute-done.14.refs_0_, bf16[2,288,256]{2,1,0:T(8,128)(2,1)S(1)} %collective-permute-done.5.refs_1_, bf16[256,512]{1,0:T(8,128)(2,1)S(1)} %get-tuple-element.18.refs_2_.refs_3_, ...), custom_call_target="tpu_custom_call" | custom-call | flops 2818572288 | bytes 4194304 | tf_op jit(solution)/shard_map/attend/pallas_call | solution.py:193
  75.9 0.8 collective-permute-start.9
  76.8 6.3 %attend.7 = (f32[16,80,256]{2,1,0:T(8,128)S(1)}, f32[16,8,256]{2,1,0:T(8,128)S(1)}) custom-call(bf16[2,288,256]{2,1,0:T(8,128)(2,1)S(1)} %collective-permute-done.10.refs_0_, bf16[2,288,256]{2,1,0:T(8,128)(2,1)S(1)} %collective-permute-done.6.refs_1_, bf16[256,512]{1,0:T(8,128)(2,1)S(1)} %get-tuple-element.18.refs_2_.refs_3_, ...), custom_call_target="tpu_custom_call" | custom-call | flops 2818572288 | bytes 4194304 | tf_op jit(solution)/shard_map/attend/pallas_call | solution.py:193
  83.1 4.9 %attend.9 = bf16[12,80,256]{2,1,0:T(8,128)(2,1)S(1)} custom-call(bf16[2,288,256]{2,1,0:T(8,128)(2,1)S(1)} %collective-permute-done.7.refs_0_, bf16[1,288,256]{2,1,0:T(8,128)(2,1)S(1)} %collective-permute-done.8.refs_1_, bf16[1,288,256]{2,1,0:T(8,128)(2,1)S(1)} %collective-permute-done.9.refs_2_, bf16[256,512]{1,0:T(8,128)(2,1)S(1)} %get-tuple-element.18.refs_2_.refs_3_, ...), custom_call_target="tpu_custom_call" | custom-call | flops 2113929216 | bytes 4194304 | tf_op jit(solution)/shard_map/attend/pallas_call | solution.py:193
  88.0 0.9 collective-permute-start.17
  89.3 2.3 %collective-permute-start.15 = (bf16[4,80,256]{2,1,0:T(8,128)(2,1)S(1)}, bf16[4,80,256]{2,1,0:T(8,128)(2,1)S(1)}, u32[]{:S(2)}, u32[]{:S(2)}) collective-permute-start(bf16[4,80,256]{2,1,0:T(8,128)(2,1)S(1)} %get-tuple-element.39), channel_id=1, source_target_pairs={{0,24},{4,28},{8,0},{12,4},{16,8},{20,12},{24,16},{28,20},{32,56},... | collective-permute-start | bytes 491528 | tf_op jit(solution)/shard_map/ppermute | solution.py:29
  91.6 0.8 fusion.45.refs_5_
  92.5 2.1 %attend.8.refs_0_ = bf16[4,80,256]{2,1,0:T(8,128)(2,1)S(1)} custom-call(bf16[2,288,256]{2,1,0:T(8,128)(2,1)S(1)} %collective-permute-done.7.refs_0_, bf16[1,288,256]{2,1,0:T(8,128)(2,1)S(1)} %collective-permute-done.8.refs_1_, bf16[1,288,256]{2,1,0:T(8,128)(2,1)S(1)} %collective-permute-done.9.refs_2_, ...), custom_call_target="tpu_custom_call" | custom-call | flops 704643072 | bytes 4194304 | tf_op jit(solution)/shard_map/attend/pallas_call | solution.py:193
  94.6 0.8 collective-permute-done.17.refs_3_
  95.4 3.9 %collective-permute-done.16.refs_2_ = bf16[4,80,256]{2,1,0:T(8,128)(2,1)S(1)} collective-permute-done((bf16[4,80,256]{2,1,0:T(8,128)(2,1)S(1)}, bf16[4,80,256]{2,1,0:T(8,128)(2,1)S(1)}, u32[]{:S(2)}, u32[]{:S(2)}) %collective-permute-start.16) | collective-permute-done | bytes 163872 | tf_op jit(solution)/shard_map/ppermute | solution.py:29
  99.3 0.6 merge.1
  99.9 1.6 %collective-permute-start.23 = (bf16[256,512]{1,0:T(8,128)(2,1)S(1)}, bf16[256,512]{1,0:T(8,128)(2,1)S(1)}, u32[]{:S(2)}, u32[]{:S(2)}) collective-permute-start(bf16[256,512]{1,0:T(8,128)(2,1)S(1)} %get-tuple-element.28), channel_id=1, source_target_pairs={{0,1},{1,2},{2,3},{3,0},{4,5},{5,6},{6,7},{7,4},{8,9},{9,10},{10,1... | collective-permute-start | bytes 786440 | tf_op jit(solution)/shard_map/ppermute | solution.py:43
  101.5 0.6 collective-permute-start.24
  102.1 1.9 %collective-permute-start.25 = (bf16[256,512]{1,0:T(8,128)(2,1)S(1)}, bf16[256,512]{1,0:T(8,128)(2,1)S(1)}, u32[]{:S(2)}, u32[]{:S(2)}) collective-permute-start(bf16[256,512]{1,0:T(8,128)(2,1)S(1)} %get-tuple-element.30), channel_id=1, source_target_pairs={{0,3},{1,0},{2,1},{3,2},{4,7},{5,4},{6,5},{7,6},{8,11},{9,8},{10,9... | collective-permute-start | bytes 786440 | tf_op jit(solution)/shard_map/ppermute | solution.py:43
  104.0 5.2 %collective-permute-done.23 = bf16[256,512]{1,0:T(8,128)(2,1)S(1)} collective-permute-done((bf16[256,512]{1,0:T(8,128)(2,1)S(1)}, bf16[256,512]{1,0:T(8,128)(2,1)S(1)}, u32[]{:S(2)}, u32[]{:S(2)}) %collective-permute-start.23) | collective-permute-done | bytes 262176 | tf_op jit(solution)/shard_map/ppermute | solution.py:43
  109.2 4.5 %collective-permute-done.24 = bf16[256,512]{1,0:T(8,128)(2,1)S(1)} collective-permute-done((bf16[256,512]{1,0:T(8,128)(2,1)S(1)}, bf16[256,512]{1,0:T(8,128)(2,1)S(1)}, u32[]{:S(2)}, u32[]{:S(2)}) %collective-permute-start.24) | collective-permute-done | bytes 262176 | tf_op jit(solution)/shard_map/ppermute | solution.py:43
  113.7 0.9 collective-permute-done.25
  114.6 0.8 add_convert_fusion
  (84 shorter events, 4.1 us)
Async XLA Ops:
  0.0 91.6 %copy-start = (bf16[512,2048]{1,0:T(8,128)(2,1)S(1)}, bf16[512,2048]{1,0:T(8,128)(2,1)}, u32[]{:S(2)}) copy-start(bf16[512,2048]{1,0:T(8,128)(2,1)} %param.35) | copy-start | bytes 6291460
  0.0 17.3 %copy-start.14 = (f32[2048]{0:T(1024)S(1)}, f32[2048]{0:T(1024)}, u32[]{:S(2)}) copy-start(f32[2048]{0:T(1024)} %param.19) | copy-start | bytes 24580
  0.0 17.3 %copy-start.13 = (bf16[2048,32]{0,1:T(8,128)(2,1)S(1)}, bf16[2048,32]{0,1:T(8,128)(2,1)}, u32[]{:S(2)}) copy-start(bf16[2048,32]{0,1:T(8,128)(2,1)} %param.22) | copy-start | bytes 393220
  0.0 9.3 %collective-permute-start.1 = (bf16[256,512]{1,0:T(8,128)(2,1)}, bf16[256,512]{1,0:T(8,128)(2,1)S(1)}, u32[]{:S(2)}, u32[]{:S(2)}) collective-permute-start(bf16[256,512]{1,0:T(8,128)(2,1)} %param.18), channel_id=1, source_target_pairs={{0,2},{1,3},{2,0},{3,1},{4,6},{5,7},{6,4},{7,5},{8,10},{9,11},{10,... | collective-permute-start | bytes 786440 | tf_op jit(solution)/shard_map/ppermute | solution.py:43
  3.7 12.0 %collective-permute-start = (bf16[256,512]{1,0:T(8,128)(2,1)}, bf16[256,512]{1,0:T(8,128)(2,1)S(1)}, u32[]{:S(2)}, u32[]{:S(2)}) collective-permute-start(bf16[256,512]{1,0:T(8,128)(2,1)} %param.18), channel_id=1, source_target_pairs={{0,3},{1,0},{2,1},{3,2},{4,7},{5,4},{6,5},{7,6},{8,11},{9,8},{10,9... | collective-permute-start | bytes 786440 | tf_op jit(solution)/shard_map/ppermute | solution.py:43
  4.5 11.4 %collective-permute-start.2 = (bf16[256,512]{1,0:T(8,128)(2,1)}, bf16[256,512]{1,0:T(8,128)(2,1)S(1)}, u32[]{:S(2)}, u32[]{:S(2)}) collective-permute-start(bf16[256,512]{1,0:T(8,128)(2,1)} %param.18), channel_id=1, source_target_pairs={{0,1},{1,2},{2,3},{3,0},{4,5},{5,6},{6,7},{7,4},{8,9},{9,10},{10,1... | collective-permute-start | bytes 786440 | tf_op jit(solution)/shard_map/ppermute | solution.py:43
  6.2 0.9 copy-start.2
  7.1 0.9 copy-start.3
  17.3 1.2 %copy-start.12 = (bf16[2048,256]{1,0:T(8,128)(2,1)S(1)}, bf16[2048,256]{1,0:T(8,128)(2,1)}, u32[]{:S(2)}) copy-start(bf16[2048,256]{1,0:T(8,128)(2,1)} %param.21) | copy-start | bytes 3145732
  18.6 0.7 copy-start.8
  18.6 2.2 %copy-start.9 = (bf16[2048,512]{1,0:T(8,128)(2,1)S(1)}, bf16[2048,512]{1,0:T(8,128)(2,1)}, u32[]{:S(2)}) copy-start(bf16[2048,512]{1,0:T(8,128)(2,1)} %param.30) | copy-start | bytes 6291460
  19.4 2.2 %copy-start.10 = (bf16[2048,512]{1,0:T(8,128)(2,1)S(1)}, bf16[2048,512]{1,0:T(8,128)(2,1)}, u32[]{:S(2)}) copy-start(bf16[2048,512]{1,0:T(8,128)(2,1)} %param.20) | copy-start | bytes 6291460
  19.4 20.5 %collective-permute-start.3 = (bf16[288,256]{1,0:T(8,128)(2,1)S(1)}, bf16[288,256]{1,0:T(8,128)(2,1)S(1)}, u32[]{:S(2)}, u32[]{:S(2)}) collective-permute-start(bf16[288,256]{1,0:T(8,128)(2,1)S(1)} %get-tuple-element.45), channel_id=1, source_target_pairs={{0,4},{4,0},{8,12},{12,8},{16,20},{20,16},{24,28},{28,24},{32,36},... | collective-permute-start | bytes 442376 | tf_op jit(solution)/shard_map/ppermute | solution.py:29
  21.6 1.6 %copy-start.11 = (bf16[2048,512]{1,0:T(8,128)(2,1)S(1)}, bf16[2048,512]{1,0:T(8,128)(2,1)}, u32[]{:S(2)}) copy-start(bf16[2048,512]{1,0:T(8,128)(2,1)} %param.29) | copy-start | bytes 6291460
  23.2 6.5 %copy-start.5 = (bf16[512,128]{1,0:T(8,128)(2,1)S(1)}, bf16[512,128]{1,0:T(8,128)(2,1)}, u32[]{:S(2)}) copy-start(bf16[512,128]{1,0:T(8,128)(2,1)} %param.26) | copy-start | bytes 393220
  23.2 6.5 %copy-start.6 = (f32[512]{0:T(512)S(1)}, f32[512]{0:T(512)}, u32[]{:S(2)}) copy-start(f32[512]{0:T(512)} %param.23) | copy-start | bytes 6148
  23.2 6.9 %copy-start.4 = (bf16[512,256]{1,0:T(8,128)(2,1)S(1)}, bf16[512,256]{1,0:T(8,128)(2,1)}, u32[]{:S(2)}) copy-start(bf16[512,256]{1,0:T(8,128)(2,1)} %param.25) | copy-start | bytes 786436
  23.9 9.0 %copy-start.7 = (f32[512]{0:T(512)S(1)}, f32[512]{0:T(512)}, u32[]{:S(2)}) copy-start(f32[512]{0:T(512)} %param.32) | copy-start | bytes 6148
  24.0 6.5 %collective-permute-start.18 = (bf16[15,512]{1,0:T(8,128)(2,1)S(1)}, bf16[15,512]{1,0:T(8,128)(2,1)S(1)}, u32[]{:S(2)}, u32[]{:S(2)}) collective-permute-start(bf16[15,512]{1,0:T(8,128)(2,1)S(1)} %get-tuple-element.40), channel_id=1, source_target_pairs={{0,4},{4,8},{8,12},{12,16},{16,20},{20,24},{24,28},{28,32},{32,36}... | collective-permute-start | bytes 46088 | tf_op jit(solution)/shard_map/ppermute | solution.py:357
  27.8 5.1 %collective-permute-start.19 = (bf16[15,512]{1,0:T(8,128)(2,1)S(1)}, bf16[15,512]{1,0:T(8,128)(2,1)S(1)}, u32[]{:S(2)}, u32[]{:S(2)}) collective-permute-start(bf16[15,512]{1,0:T(8,128)(2,1)S(1)} %get-tuple-element.41), channel_id=1, source_target_pairs={{4,0},{8,4},{12,8},{16,12},{20,16},{24,20},{28,24},{32,28},{36,32}... | collective-permute-start | bytes 46088 | tf_op jit(solution)/shard_map/ppermute | solution.py:358
  35.8 12.6 %collective-permute-start.21 = (f32[2,256]{1,0:T(2,128)S(1)}, f32[2,256]{1,0:T(2,128)S(1)}, u32[]{:S(2)}, u32[]{:S(2)}) collective-permute-start(f32[2,256]{1,0:T(2,128)S(1)} %get-tuple-element.80), channel_id=1, source_target_pairs={{0,3},{1,0},{2,1},{3,2},{4,7},{5,4},{6,5},{7,6},{8,11},{9,8},{10,9... | collective-permute-start | bytes 6152 | tf_op jit(solution)/shard_map/ppermute | solution.py:43
  38.2 11.2 %collective-permute-start.20 = (f32[2,256]{1,0:T(2,128)S(1)}, f32[2,256]{1,0:T(2,128)S(1)}, u32[]{:S(2)}, u32[]{:S(2)}) collective-permute-start(f32[2,256]{1,0:T(2,128)S(1)} %get-tuple-element.80), channel_id=1, source_target_pairs={{0,1},{1,2},{2,3},{3,0},{4,5},{5,6},{6,7},{7,4},{8,9},{9,10},{10,1... | collective-permute-start | bytes 6152 | tf_op jit(solution)/shard_map/ppermute | solution.py:43
  38.2 11.6 %collective-permute-start.22 = (f32[2,256]{1,0:T(2,128)S(1)}, f32[2,256]{1,0:T(2,128)S(1)}, u32[]{:S(2)}, u32[]{:S(2)}) collective-permute-start(f32[2,256]{1,0:T(2,128)S(1)} %get-tuple-element.80), channel_id=1, source_target_pairs={{0,2},{1,3},{2,0},{3,1},{4,6},{5,7},{6,4},{7,5},{8,10},{9,11},{10,... | collective-permute-start | bytes 6152 | tf_op jit(solution)/shard_map/ppermute | solution.py:43
  39.9 9.9 %collective-permute-start.4 = (bf16[2,288,256]{2,1,0:T(8,128)(2,1)S(1)}, bf16[2,288,256]{2,1,0:T(8,128)(2,1)S(1)}, u32[]{:S(2)}, u32[]{:S(2)}) collective-permute-start(bf16[2,288,256]{2,1,0:T(8,128)(2,1)S(1)} %pad_maximum_fusion.1.refs_0_), channel_id=1, source_target_pairs={{0,32},{4,228},{8,40},{12,236},{16,48},{20,244},{24,56},{28,252},{... | collective-permute-start | bytes 884744 | tf_op jit(solution)/shard_map/ppermute | solution.py:38
  45.6 13.9 %collective-permute-start.13 = (bf16[384,256]{1,0:T(8,128)(2,1)S(1)}, bf16[384,256]{1,0:T(8,128)(2,1)S(1)}, u32[]{:S(2)}, u32[]{:S(2)}) collective-permute-start(bf16[384,256]{1,0:T(8,128)(2,1)S(1)} %bitcast.66), channel_id=1, source_target_pairs={{0,16},{4,20},{8,24},{12,28},{16,0},{20,4},{24,8},{28,12},{32,48},... | collective-permute-start | bytes 589832 | tf_op jit(solution)/shard_map/ppermute | solution.py:29
  48.3 12.1 %collective-permute-start.12 = (bf16[384,256]{1,0:T(8,128)(2,1)S(1)}, bf16[384,256]{1,0:T(8,128)(2,1)S(1)}, u32[]{:S(2)}, u32[]{:S(2)}) collective-permute-start(bf16[384,256]{1,0:T(8,128)(2,1)S(1)} %bitcast.67), channel_id=1, source_target_pairs={{0,24},{4,28},{8,0},{12,4},{16,8},{20,12},{24,16},{28,20},{32,56},... | collective-permute-start | bytes 589832 | tf_op jit(solution)/shard_map/ppermute | solution.py:29
  49.4 11.0 %collective-permute-start.11 = (bf16[384,256]{1,0:T(8,128)(2,1)S(1)}, bf16[384,256]{1,0:T(8,128)(2,1)S(1)}, u32[]{:S(2)}, u32[]{:S(2)}) collective-permute-start(bf16[384,256]{1,0:T(8,128)(2,1)S(1)} %bitcast.68), channel_id=1, source_target_pairs={{0,8},{4,12},{8,16},{12,20},{16,24},{20,28},{24,0},{28,4},{32,40},... | collective-permute-start | bytes 589832 | tf_op jit(solution)/shard_map/ppermute | solution.py:29
  49.9 6.5 %collective-permute-start.5 = (bf16[2,288,256]{2,1,0:T(8,128)(2,1)S(1)}, bf16[2,288,256]{2,1,0:T(8,128)(2,1)S(1)}, u32[]{:S(2)}, u32[]{:S(2)}) collective-permute-start(bf16[2,288,256]{2,1,0:T(8,128)(2,1)S(1)} %collective-permute-done.4.refs_1_), channel_id=1, source_target_pairs={{0,32},{4,228},{8,40},{12,236},{16,48},{20,244},{24,56},{28,252},{... | collective-permute-start | bytes 884744 | tf_op jit(solution)/shard_map/ppermute | solution.py:38
  52.7 16.9 %collective-permute-start.14 = (bf16[2,288,256]{2,1,0:T(8,128)(2,1)S(1)}, bf16[2,288,256]{2,1,0:T(8,128)(2,1)S(1)}, u32[]{:S(2)}, u32[]{:S(2)}) collective-permute-start(bf16[2,288,256]{2,1,0:T(8,128)(2,1)S(1)} %collective-permute-done.4.refs_1_), channel_id=1, source_target_pairs={{0,4},{4,0},{8,12},{12,8},{16,20},{20,16},{24,28},{28,24},{32,36},... | collective-permute-start | bytes 884744 | tf_op jit(solution)/shard_map/ppermute | solution.py:29
  56.3 10.3 %collective-permute-start.6 = (bf16[2,288,256]{2,1,0:T(8,128)(2,1)S(1)}, bf16[2,288,256]{2,1,0:T(8,128)(2,1)S(1)}, u32[]{:S(2)}, u32[]{:S(2)}) collective-permute-start(bf16[2,288,256]{2,1,0:T(8,128)(2,1)S(1)} %collective-permute-done.5.refs_1_), channel_id=1, source_target_pairs={{0,32},{4,228},{8,40},{12,236},{16,48},{20,244},{24,56},{28,252},{... | collective-permute-start | bytes 884744 | tf_op jit(solution)/shard_map/ppermute | solution.py:38
  59.5 17.3 %collective-permute-start.10 = (bf16[2,288,256]{2,1,0:T(8,128)(2,1)S(1)}, bf16[2,288,256]{2,1,0:T(8,128)(2,1)S(1)}, u32[]{:S(2)}, u32[]{:S(2)}) collective-permute-start(bf16[2,288,256]{2,1,0:T(8,128)(2,1)S(1)} %collective-permute-done.5.refs_1_), channel_id=1, source_target_pairs={{0,4},{4,0},{8,12},{12,8},{16,20},{20,16},{24,28},{28,24},{32,36},... | collective-permute-start | bytes 884744 | tf_op jit(solution)/shard_map/ppermute | solution.py:29
  66.6 9.3 %collective-permute-start.8 = (bf16[1,288,256]{2,1,0:T(8,128)(2,1)S(1)}, bf16[1,288,256]{2,1,0:T(8,128)(2,1)S(1)}, u32[]{:S(2)}, u32[]{:S(2)}) collective-permute-start(bf16[1,288,256]{2,1,0:T(8,128)(2,1)S(1)} %slice.302), channel_id=1, source_target_pairs={{0,32},{4,228},{8,40},{12,236},{16,48},{20,244},{24,56},{28,252},{... | collective-permute-start | bytes 442376 | tf_op jit(solution)/shard_map/ppermute | solution.py:38
  69.6 13.5 %collective-permute-start.7 = (bf16[2,288,256]{2,1,0:T(8,128)(2,1)S(1)}, bf16[2,288,256]{2,1,0:T(8,128)(2,1)S(1)}, u32[]{:S(2)}, u32[]{:S(2)}) collective-permute-start(bf16[2,288,256]{2,1,0:T(8,128)(2,1)S(1)} %collective-permute-done.6.refs_1_), channel_id=1, source_target_pairs={{0,4},{4,0},{8,12},{12,8},{16,20},{20,16},{24,28},{28,24},{32,36},... | collective-permute-start | bytes 884744 | tf_op jit(solution)/shard_map/ppermute | solution.py:29
  75.9 7.2 %collective-permute-start.9 = (bf16[1,288,256]{2,1,0:T(8,128)(2,1)S(1)}, bf16[1,288,256]{2,1,0:T(8,128)(2,1)S(1)}, u32[]{:S(2)}, u32[]{:S(2)}) collective-permute-start(bf16[1,288,256]{2,1,0:T(8,128)(2,1)S(1)} %collective-permute-done.8.refs_1_), channel_id=1, source_target_pairs={{0,4},{4,0},{8,12},{12,8},{16,20},{20,16},{24,28},{28,24},{32,36},... | collective-permute-start | bytes 442376 | tf_op jit(solution)/shard_map/ppermute | solution.py:29
  83.1 8.5 %copy-start.15 = (f32[512]{0:T(512)S(1)}, f32[512]{0:T(512)}, u32[]{:S(2)}) copy-start(f32[512]{0:T(512)} %param.33) | copy-start | bytes 6148
  88.0 7.4 %collective-permute-start.17 = (bf16[4,80,256]{2,1,0:T(8,128)(2,1)S(1)}, bf16[4,80,256]{2,1,0:T(8,128)(2,1)S(1)}, u32[]{:S(2)}, u32[]{:S(2)}) collective-permute-start(bf16[4,80,256]{2,1,0:T(8,128)(2,1)S(1)} %get-tuple-element.37), channel_id=1, source_target_pairs={{0,16},{4,20},{8,24},{12,28},{16,0},{20,4},{24,8},{28,12},{32,48},... | collective-permute-start | bytes 491528 | tf_op jit(solution)/shard_map/ppermute | solution.py:29
  88.9 10.3 %collective-permute-start.16 = (bf16[4,80,256]{2,1,0:T(8,128)(2,1)S(1)}, bf16[4,80,256]{2,1,0:T(8,128)(2,1)S(1)}, u32[]{:S(2)}, u32[]{:S(2)}) collective-permute-start(bf16[4,80,256]{2,1,0:T(8,128)(2,1)S(1)} %get-tuple-element.38), channel_id=1, source_target_pairs={{0,8},{4,12},{8,16},{12,20},{16,24},{20,28},{24,0},{28,4},{32,40},... | collective-permute-start | bytes 491528 | tf_op jit(solution)/shard_map/ppermute | solution.py:29
  89.3 9.9 %collective-permute-start.15 = (bf16[4,80,256]{2,1,0:T(8,128)(2,1)S(1)}, bf16[4,80,256]{2,1,0:T(8,128)(2,1)S(1)}, u32[]{:S(2)}, u32[]{:S(2)}) collective-permute-start(bf16[4,80,256]{2,1,0:T(8,128)(2,1)S(1)} %get-tuple-element.39), channel_id=1, source_target_pairs={{0,24},{4,28},{8,0},{12,4},{16,8},{20,12},{24,16},{28,20},{32,56},... | collective-permute-start | bytes 491528 | tf_op jit(solution)/shard_map/ppermute | solution.py:29
  92.5 6.8 %copy-start.1 = (bf16[256,2048]{1,0:T(8,128)(2,1)S(1)}, bf16[256,2048]{1,0:T(8,128)(2,1)}, u32[]{:S(2)}) copy-start(bf16[256,2048]{1,0:T(8,128)(2,1)} %refs_4_.1) | copy-start | bytes 3145732
  99.9 9.3 %collective-permute-start.23 = (bf16[256,512]{1,0:T(8,128)(2,1)S(1)}, bf16[256,512]{1,0:T(8,128)(2,1)S(1)}, u32[]{:S(2)}, u32[]{:S(2)}) collective-permute-start(bf16[256,512]{1,0:T(8,128)(2,1)S(1)} %get-tuple-element.28), channel_id=1, source_target_pairs={{0,1},{1,2},{2,3},{3,0},{4,5},{5,6},{6,7},{7,4},{8,9},{9,10},{10,1... | collective-permute-start | bytes 786440 | tf_op jit(solution)/shard_map/ppermute | solution.py:43
  101.5 12.2 %collective-permute-start.24 = (bf16[256,512]{1,0:T(8,128)(2,1)S(1)}, bf16[256,512]{1,0:T(8,128)(2,1)S(1)}, u32[]{:S(2)}, u32[]{:S(2)}) collective-permute-start(bf16[256,512]{1,0:T(8,128)(2,1)S(1)} %get-tuple-element.29), channel_id=1, source_target_pairs={{0,2},{1,3},{2,0},{3,1},{4,6},{5,7},{6,4},{7,5},{8,10},{9,11},{10,... | collective-permute-start | bytes 786440 | tf_op jit(solution)/shard_map/ppermute | solution.py:43
  102.1 12.5 %collective-permute-start.25 = (bf16[256,512]{1,0:T(8,128)(2,1)S(1)}, bf16[256,512]{1,0:T(8,128)(2,1)S(1)}, u32[]{:S(2)}, u32[]{:S(2)}) collective-permute-start(bf16[256,512]{1,0:T(8,128)(2,1)S(1)} %get-tuple-element.30), channel_id=1, source_target_pairs={{0,3},{1,0},{2,1},{3,2},{4,7},{5,4},{6,5},{7,6},{8,11},{9,8},{10,9... | collective-permute-start | bytes 786440 | tf_op jit(solution)/shard_map/ppermute | solution.py:43

commit v2 on v1

--- a/solution.py
+++ b/solution.py
@@ -41,6 +41,12 @@
 def moved_tp(values, step):
     count = lax.axis_size("tp")
     return lax.ppermute(values, "tp", [(i, (i + step) % count) for i in range(count)])
+
+
+def over_edge(values):
+    count = lax.axis_size("sp")
+    pairs = [(i, i + 1 if i % 2 else i - 1) for i in range(count) if 0 < i < count - 1]
+    return lax.ppermute(values, "sp", pairs)
 
 
 def in_order(me, came):
@@ -153,24 +159,32 @@
         tail = jnp.where(row == 0, total_high, jnp.where(row == 1, total - total_high, top))
         out[i] = jnp.concatenate([o[:vdim], tail, tail], axis=0).astype(bf16)
 
-    scores(0, sa, ma)
-    scores(1, sb, mb)
-    weights(sa, ma, pa)
+    def score_pair(i):
+        scores(i, sa, ma)
+        scores(i + 1, sb, mb)
+
+    def weight_pair():
+        weights(sa, ma, pa)
+        weights(sb, mb, pb)
+
+    def value_pair(i):
+        values(i, pa)
+        values(i + 1, pb)
+
+    score_pair(0)
+    weight_pair()
+    score_pair(2)
 
     def step(j, carry):
-        i = 2 * j
-        scores(i + 2, sa, ma)
-        weights(sb, mb, pb)
-        values(i, pa)
-        scores(i + 3, sb, mb)
-        weights(sa, ma, pa)
-        values(i + 1, pb)
+        value_pair(2 * j)
+        weight_pair()
+        score_pair(2 * j + 4)
         return carry
 
-    lax.fori_loop(0, items // 2 - 1, step, 0)
-    weights(sb, mb, pb)
-    values(items - 2, pa)
-    values(items - 1, pb)
+    lax.fori_loop(0, items // 2 - 2, step, 0)
+    value_pair(items - 4)
+    weight_pair()
+    value_pair(items - 2)
 
 
 def attend(lat, kup, vup, place, q, heads, scale, state=None, last=False, skip=0):
@@ -312,11 +326,28 @@
     score_scale = (nope + rope_size) ** -0.5 * math.log2(math.e)
 
     me = lax.axis_index("tp")
-    came = [tokens] + [moved_tp(tokens, step) for step in (-1, 2, 1)]
-    piece_f = jnp.concatenate(in_order(me, came), axis=1).astype(f32)
-    scaled = (piece_f * in_gain).astype(bf16)
-    square_sum = jnp.sum(piece_f * piece_f, axis=1)
-    row_scale = lax.rsqrt(square_sum / width + eps_norm)[:, None]
+    taps = conv_taps.shape[0]
+    reach = taps // 2
+    edge = (reach + 15) // 16 * 16
+
+    def gathered(own):
+        came = [own] + [moved_tp(own, step) for step in (-1, 2, 1)]
+        return jnp.concatenate(in_order(me, came), axis=1).astype(f32)
+
+    def normed(piece):
+        return (piece * in_gain).astype(bf16), lax.rsqrt(
+            jnp.sum(piece * piece, axis=1) / width + eps_norm
+        )[:, None]
+
+    whole = gathered(tokens)
+    scaled, row_scale = normed(whole)
+
+    even = lax.rem(sp, 2) == 0
+    head, tail = tokens[:edge], tokens[row_count - edge :]
+    near = moved(jnp.where(even, tail, head), dc=1)
+    across = over_edge(jnp.where(even, head, tail))
+    ends = jnp.concatenate([jnp.where(even, across, near), jnp.where(even, near, across)], axis=0)
+    scaled_ends, scale_ends = normed(gathered(ends))
 
     def add_rows(weight):
         return jnp.dot(scaled, weight, preferred_element_type=f32)
@@ -324,7 +355,8 @@
     kv_latent = rms_scale(row_scale * add_rows(latent_down), latent_gain).astype(bf16)
     rope_key = rotate_rows(columns(rope_down, scaled) * row_scale[:, 0], positions).astype(bf16)
     lat = jnp.concatenate([kv_latent, rope_key], axis=0)
-    q_latent = rms_scale(row_scale * add_rows(query_down), query_gain).astype(bf16)
+    q_pre = add_rows(query_down)
+    q_latent = rms_scale(row_scale * q_pre, query_gain).astype(bf16)
     q_flat = columns(query_nope, q_latent).astype(bf16).reshape(heads, nope, row_count)
     q_turn = columns(query_rope, q_latent).reshape(heads, rope_size, row_count)
     r_flat = rotate_rows(q_turn, positions).astype(bf16)
@@ -348,25 +380,30 @@
             blocks, kup, vup, place, queries, heads, score_scale, state, last, skip
         )
 
+    wide = jnp.concatenate([scaled_ends[:edge], scaled, scaled_ends[edge:]], axis=0)
+    wide_scale = jnp.concatenate([scale_ends[:edge], row_scale, scale_ends[edge:]], axis=0)
     glu = (
-        row_scale * add_rows(conv_value) * jax.nn.sigmoid(row_scale * add_rows(conv_gate))
-    ).astype(bf16)
-    taps = conv_taps.shape[0]
-    reach = taps // 2
-    count = lax.axis_size("sp")
-    before = lax.ppermute(glu[row_count - reach :], "sp", [(i, i + 1) for i in range(count - 1)])
-    after = lax.ppermute(glu[:reach], "sp", [(i + 1, i) for i in range(count - 1)])
-    padded = jnp.concatenate([before, glu, after], axis=0).astype(f32)
+        wide_scale
+        * jnp.dot(wide, conv_value, preferred_element_type=f32)
+        * jax.nn.sigmoid(wide_scale * jnp.dot(wide, conv_gate, preferred_element_type=f32))
+    )
+    glu = lax.reduce_precision(glu, 8, 7)
+    padded = glu[edge - reach : edge + row_count + reach]
     conv = jnp.zeros((row_count, local_ch), f32) + conv_bias
     for tap in range(taps):
         conv = conv + conv_taps[tap] * padded[tap : tap + row_count]
     own_mean = jnp.mean(conv, axis=-1)
     own_off = conv - own_mean[:, None]
-    own_stats = jnp.stack([own_mean, jnp.sum(own_off * own_off, axis=-1)])
-    stats = jnp.stack([own_stats] + [moved_tp(own_stats, k) for k in (1, -1, 2)])
-    mean = jnp.mean(stats[:, 0], axis=0)
-    apart = stats[:, 0] - mean
-    spread = jnp.sum(stats[:, 1] + local_ch * apart * apart, axis=0) / (4 * local_ch)
+    own_square = jnp.sum(own_off * own_off, axis=-1)
+    mean, square, channels = own_mean, own_square, local_ch
+    for step in (1, 2):
+        pairs = [(i, i ^ step) for i in range(4)]
+        other = lax.ppermute(jnp.stack([mean, square]), "tp", pairs)
+        apart = other[0] - mean
+        mean = (mean + other[0]) * 0.5
+        square = square + other[1] + apart * apart * (channels * 0.5)
+        channels *= 2
+    spread = square / channels
     activated = jax.nn.silu(
         (conv - mean[:, None]) * lax.rsqrt(spread + eps_layer)[:, None] * channel_gain
     ).astype(bf16)
@@ -377,12 +414,12 @@
     state = part([own, hop1], own_first)
     state = part([side1, hop2], own_first, state)
     state = part([side2, hop3], own_first, state)
-    ends = [side3, hop4, side4]
-    (packed,) = part(ends, q_far, state, True, heads)
+    rest = [side3, hop4, side4]
+    (packed,) = part(rest, q_far, state, True, heads)
     packed = packed.reshape((3, heads) + packed.shape[1:])
 
     parts = [moved(packed[k], dy=d) for k, d in enumerate((-1, 1, 2))]
-    (packed_own,) = part(ends, [q_own], state, True)
+    (packed_own,) = part(rest, [q_own], state, True)
     cuts = merge(me, [packed_own] + parts, out_attend, conv_part)
     mixed = cuts[0].astype(f32)
     for k, step in ((1, 1), (2, 2), (3, -1)):

time: 116 us -> 113 us (0.974)
  waiting for transfers between devices: 27.9 us -> 24.5 us
  Pallas kernels: 26.5 us -> 23.4 us
  other arithmetic: 5.51 us -> 7.32 us
  starting transfers between devices: 44.5 us -> 46 us
    pallas_call x5, Pallas kernels: 25.8 us -> 22.6 us  [attend(): pl.pallas_call(functools.partial(attend_kernel, sizes, nq, heads, first,...]
    ppermute x11 -> x12, waiting for transfers between devices: 4.71 us -> 7.52 us  [moved(): return lax.ppermute(values, 'sp', pairs)]
    ppermute x2 -> x3, waiting for transfers between devices: 2.4 us -> 0.01 us  [the longest x2 0.01 us: per_device(): other = lax.ppermute(jnp.stack([mean, square]), 'tp', pairs)]
    ppermute x9, waiting for transfers between devices: 17.3 us -> 15 us  [moved_tp(): lax.ppermute(values, 'tp', [(i, (i + step) % count) for i in range(count)])]
    ppermute x2 -> x3, starting transfers between devices: 5.75 us -> 7.53 us  [the longest x1 4.31 us: over_edge(): return lax.ppermute(values, 'sp', pairs)]
    dot_general x0 -> x2, matrix products: none -> 1.68 us  [the longest x1 0.88 us: per_device(): jnp.dot(wide, conv_gate, preferred_element_type=f32)]
    ppermute x4, waiting for transfers between devices: 3.56 us -> 1.96 us  [passed_on(): return lax.ppermute(values, 'sp', pairs)]
    dot_general x4 -> x2, matrix products: 2.88 us -> 1.32 us  [add_rows(): return jnp.dot(scaled, weight, preferred_element_type=f32)]
  transfers between devices with their start and end apart: 26 -> 28, of which waited for: 9 -> 11; matrix products, arithmetic and copies ran while one was open for 8% -> 10% of each run, Pallas kernels for 18% -> 17%
where the time goes in v2:
time: 113 us; the launch traced here: 112 us
  starting transfers between devices  46 us (41%)
  waiting for transfers between devices  24.5 us (22%)
  Pallas kernels  23.4 us (21%)
  other arithmetic  7.32 us (6%)
  local copies, waits for them, and re-layouts  5.22 us (5%)
  matrix products  4.9 us (4%)
    pallas_call x5, Pallas kernels, attend(): pl.pallas_call(functools.partial(attend_kernel, sizes, nq, heads, first,...  22.6 us
    ppermute x9, waiting for transfers between devices, moved_tp(): lax.ppermute(values, 'tp', [(i, (i + step) % count) for i in range(count)])  15 us
    ppermute x4, starting transfers between devices, passed_on(): return lax.ppermute(values, 'sp', pairs)  13.9 us
    ppermute x12, starting transfers between devices, moved(): return lax.ppermute(values, 'sp', pairs)  12.3 us
    ppermute x9, starting transfers between devices, moved_tp(): lax.ppermute(values, 'tp', [(i, (i + step) % count) for i in range(count)])  12.2 us
    ppermute x12, waiting for transfers between devices, moved(): return lax.ppermute(values, 'sp', pairs)  7.52 us
    ppermute x1, starting transfers between devices, over_edge(): return lax.ppermute(values, 'sp', pairs)  4.31 us
    ppermute x2, starting transfers between devices, per_device(): other = lax.ppermute(jnp.stack([mean, square]), 'tp', pairs)  3.22 us
  transfers between devices with their start and end apart: 28, of which 11 were waited for; matrix products, arithmetic and copies ran while one was open for 10% of the time, Pallas kernels for 17%

profile of v2, /device:TPU:1, one launch (start us, length us, event | category | flops | bytes accessed | tf_op | source)
XLA Modules:
  0.0 111.8 jit_solution(5722563506214138369)
XLA Ops:
  0.0 2.0 %collective-permute-start.2 = (bf16[256,512]{1,0:T(8,128)(2,1)}, bf16[256,512]{1,0:T(8,128)(2,1)S(1)}, u32[]{:S(2)}, u32[]{:S(2)}) collective-permute-start(bf16[256,512]{1,0:T(8,128)(2,1)} %param.18), channel_id=1, source_target_pairs={{0,1},{1,2},{2,3},{3,0},{4,5},{5,6},{6,7},{7,4},{8,9},{9,10},{10,1... | collective-permute-start | bytes 786440 | tf_op jit(solution)/shard_map/ppermute | solution.py:43
  2.0 2.5 %collective-permute-start.1 = (bf16[256,512]{1,0:T(8,128)(2,1)}, bf16[256,512]{1,0:T(8,128)(2,1)S(1)}, u32[]{:S(2)}, u32[]{:S(2)}) collective-permute-start(bf16[256,512]{1,0:T(8,128)(2,1)} %param.18), channel_id=1, source_target_pairs={{0,2},{1,3},{2,0},{3,1},{4,6},{5,7},{6,4},{7,5},{8,10},{9,11},{10,... | collective-permute-start | bytes 786440 | tf_op jit(solution)/shard_map/ppermute | solution.py:43
  4.5 0.8 broadcast_select_fusion.3
  5.2 4.3 %collective-permute-start.18 = (bf16[16,512]{1,0:T(8,128)(2,1)S(1)}, bf16[16,512]{1,0:T(8,128)(2,1)S(1)}, u32[]{:S(2)}, u32[]{:S(2)}) collective-permute-start(bf16[16,512]{1,0:T(8,128)(2,1)S(1)} %get-tuple-element.42), channel_id=1, source_target_pairs={{4,8},{8,4},{12,16},{16,12},{20,24},{24,20},{28,32},{32,28},{36,40... | collective-permute-start | bytes 49160 | tf_op jit(solution)/shard_map/ppermute | solution.py:49
  9.7 1.0 fusion.57
  10.7 1.2 %fusion.56 = (f32[1,512]{1,0:T(1,128)S(1)}, f32[1,512]{1,0:T(1,128)S(1)}, f32[1,512]{1,0:T(1,128)S(1)}, f32[1,512]{1,0:T(1,128)S(1)}, f32[1,512]{1,0:T(1,128)S(1...) fusion(f32[31,512]{1,0:T(8,128)} %param.31), kind=kLoop, calls=%fused_computation.145 | loop fusion | bytes 77824 | tf_op jit(solution)/shard_map/slice | solution.py:394
  12.0 2.3 %collective-permute-start.21 = (bf16[32,512]{1,0:T(8,128)(2,1)S(1)}, bf16[32,512]{1,0:T(8,128)(2,1)S(1)}, u32[]{:S(2)}, u32[]{:S(2)}) collective-permute-start(bf16[32,512]{1,0:T(8,128)(2,1)S(1)} %pad_maximum_fusion.8), channel_id=1, source_target_pairs={{0,2},{1,3},{2,0},{3,1},{4,6},{5,7},{6,4},{7,5},{8,10},{9,11},{10,... | collective-permute-start | bytes 98312 | tf_op jit(solution)/shard_map/ppermute | solution.py:43
  14.7 0.9 copy-done.2
  15.6 0.9 copy-done.3
  16.7 0.7 collective-permute-start
  17.5 0.8 fusion.41
  18.5 4.5 %collective-permute-done = bf16[256,512]{1,0:T(8,128)(2,1)S(1)} collective-permute-done((bf16[256,512]{1,0:T(8,128)(2,1)}, bf16[256,512]{1,0:T(8,128)(2,1)S(1)}, u32[]{:S(2)}, u32[]{:S(2)}) %collective-permute-start) | collective-permute-done | bytes 262176 | tf_op jit(solution)/shard_map/ppermute | solution.py:43
  22.9 1.1 select_select_fusion.3
  26.1 2.8 %collective-permute-start.3 = (bf16[288,256]{1,0:T(8,128)(2,1)S(1)}, bf16[288,256]{1,0:T(8,128)(2,1)S(1)}, u32[]{:S(2)}, u32[]{:S(2)}) collective-permute-start(bf16[288,256]{1,0:T(8,128)(2,1)S(1)} %get-tuple-element.47), channel_id=1, source_target_pairs={{0,4},{4,0},{8,12},{12,8},{16,20},{20,16},{24,28},{28,24},{32,36},... | collective-permute-start | bytes 442376 | tf_op jit(solution)/shard_map/ppermute | solution.py:29
  29.0 0.8 multiply_reduce_fusion.1
  30.6 0.9 fusion.7
  31.5 0.7 copy-done.13
  32.2 0.8 fusion.5
  33.0 2.6 %fusion.52 = (f32[256]{0:T(256)S(1)}, f32[256,512]{1,0:T(8,128)S(1)}) fusion(f32[288,512]{1,0:T(8,128)S(1)} %fusion.5, f32[512]{0:T(512)S(1)} %bitcast.91, f32[512]{0:T(512)S(1)} %bitcast.92, f32[512]{0:T(512)S(1)} %bitcast.94, f32[512]{0:T(512)S(1)} %bitcast.95, f32[512]{0:T(512)S(1)} %bitcast.96, f32[512]{0:T(512)S(1)} %bitcast.97, f32[512]{0:T(512)S(1)} %bitcast.98, ...), kind=kLoop, calls=%fused_computation.142 | loop fusion | flops 8257280 | bytes 16843776 | tf_op jit(solution)/shard_map/reduce_sum | solution.py:395
  35.8 1.2 %collective-permute-start.23 = (f32[2,256]{1,0:T(2,128)S(1)}, f32[2,256]{1,0:T(2,128)S(1)}, u32[]{:S(2)}, u32[]{:S(2)}) collective-permute-start(f32[2,256]{1,0:T(2,128)S(1)} %pad_maximum_fusion.9), channel_id=1, source_target_pairs={{0,1},{1,0},{2,3},{3,2},{4,5},{5,4},{6,7},{7,6},{8,9},{9,8},{10,11... | collective-permute-start | bytes 6152 | tf_op jit(solution)/shard_map/ppermute | solution.py:401
  37.1 7.0 %collective-permute-start.4 = (bf16[2,288,256]{2,1,0:T(8,128)(2,1)S(1)}, bf16[2,288,256]{2,1,0:T(8,128)(2,1)S(1)}, u32[]{:S(2)}, u32[]{:S(2)}) collective-permute-start(bf16[2,288,256]{2,1,0:T(8,128)(2,1)S(1)} %pad_maximum_fusion.4.refs_0_), channel_id=1, source_target_pairs={{0,32},{4,228},{8,40},{12,236},{16,48},{20,244},{24,56},{28,252},{... | collective-permute-start | bytes 884744 | tf_op jit(solution)/shard_map/ppermute | solution.py:38
  44.1 2.0 %collective-permute-start.24 = (f32[2,256]{1,0:T(2,128)S(1)}, f32[2,256]{1,0:T(2,128)S(1)}, u32[]{:S(2)}, u32[]{:S(2)}) collective-permute-start(f32[2,256]{1,0:T(2,128)S(1)} %pad_maximum_fusion.10), channel_id=1, source_target_pairs={{0,2},{1,3},{2,0},{3,1},{4,6},{5,7},{6,4},{7,5},{8,10},{9,11},{10,... | collective-permute-start | bytes 6152 | tf_op jit(solution)/shard_map/ppermute | solution.py:401
  46.1 1.6 %collective-permute-done.4.refs_1_ = bf16[2,288,256]{2,1,0:T(8,128)(2,1)S(1)} collective-permute-done((bf16[2,288,256]{2,1,0:T(8,128)(2,1)S(1)}, bf16[2,288,256]{2,1,0:T(8,128)(2,1)S(1)}, u32[]{:S(2)}, u32[]{:S(2)}) %collective-permute-start.4) | collective-permute-done | bytes 294944 | tf_op jit(solution)/shard_map/ppermute | solution.py:38
  47.7 3.3 %collective-permute-start.5 = (bf16[2,288,256]{2,1,0:T(8,128)(2,1)S(1)}, bf16[2,288,256]{2,1,0:T(8,128)(2,1)S(1)}, u32[]{:S(2)}, u32[]{:S(2)}) collective-permute-start(bf16[2,288,256]{2,1,0:T(8,128)(2,1)S(1)} %collective-permute-done.4.refs_1_), channel_id=1, source_target_pairs={{0,32},{4,228},{8,40},{12,236},{16,48},{20,244},{24,56},{28,252},{... | collective-permute-start | bytes 884744 | tf_op jit(solution)/shard_map/ppermute | solution.py:38
  51.0 1.8 %collective-permute-start.13 = (bf16[384,256]{1,0:T(8,128)(2,1)S(1)}, bf16[384,256]{1,0:T(8,128)(2,1)S(1)}, u32[]{:S(2)}, u32[]{:S(2)}) collective-permute-start(bf16[384,256]{1,0:T(8,128)(2,1)S(1)} %bitcast.66), channel_id=1, source_target_pairs={{0,16},{4,20},{8,24},{12,28},{16,0},{20,4},{24,8},{28,12},{32,48},... | collective-permute-start | bytes 589832 | tf_op jit(solution)/shard_map/ppermute | solution.py:29
  52.9 0.8 collective-permute-start.12
  53.7 0.6 collective-permute-start.11
  54.7 3.4 %collective-permute-start.6 = (bf16[2,288,256]{2,1,0:T(8,128)(2,1)S(1)}, bf16[2,288,256]{2,1,0:T(8,128)(2,1)S(1)}, u32[]{:S(2)}, u32[]{:S(2)}) collective-permute-start(bf16[2,288,256]{2,1,0:T(8,128)(2,1)S(1)} %collective-permute-done.5.refs_1_), channel_id=1, source_target_pairs={{0,32},{4,228},{8,40},{12,236},{16,48},{20,244},{24,56},{28,252},{... | collective-permute-start | bytes 884744 | tf_op jit(solution)/shard_map/ppermute | solution.py:38
  58.1 1.1 %collective-permute-done.13.refs_8_ = bf16[384,256]{1,0:T(8,128)(2,1)S(1)} collective-permute-done((bf16[384,256]{1,0:T(8,128)(2,1)S(1)}, bf16[384,256]{1,0:T(8,128)(2,1)S(1)}, u32[]{:S(2)}, u32[]{:S(2)}) %collective-permute-start.13) | collective-permute-done | bytes 196640 | tf_op jit(solution)/shard_map/ppermute | solution.py:29
  59.3 2.6 %collective-permute-done.12.refs_7_ = bf16[384,256]{1,0:T(8,128)(2,1)S(1)} collective-permute-done((bf16[384,256]{1,0:T(8,128)(2,1)S(1)}, bf16[384,256]{1,0:T(8,128)(2,1)S(1)}, u32[]{:S(2)}, u32[]{:S(2)}) %collective-permute-start.12) | collective-permute-done | bytes 196640 | tf_op jit(solution)/shard_map/ppermute | solution.py:29
  61.8 0.7 collective-permute-done.11.refs_6_
  62.6 5.4 %attend.5 = (f32[16,80,256]{2,1,0:T(8,128)S(1)}, f32[16,8,256]{2,1,0:T(8,128)S(1)}) custom-call(bf16[2,288,256]{2,1,0:T(8,128)(2,1)S(1)} %pad_maximum_fusion.4.refs_0_, bf16[2,288,256]{2,1,0:T(8,128)(2,1)S(1)} %collective-permute-done.4.refs_1_, bf16[256,512]{1,0:T(8,128)(2,1)S(1)} %get-tuple-element.18.refs_2_.refs_3_, ...), custom_call_target="tpu_custom_call" | custom-call | flops 2818572288 | bytes 4194304 | tf_op jit(solution)/shard_map/attend/pallas_call | solution.py:207
  68.3 5.5 %attend.6 = (f32[16,80,256]{2,1,0:T(8,128)S(1)}, f32[16,8,256]{2,1,0:T(8,128)S(1)}) custom-call(bf16[2,288,256]{2,1,0:T(8,128)(2,1)S(1)} %collective-permute-done.14.refs_0_, bf16[2,288,256]{2,1,0:T(8,128)(2,1)S(1)} %collective-permute-done.5.refs_1_, bf16[256,512]{1,0:T(8,128)(2,1)S(1)} %get-tuple-element.18.refs_2_.refs_3_, ...), custom_call_target="tpu_custom_call" | custom-call | flops 2818572288 | bytes 4194304 | tf_op jit(solution)/shard_map/attend/pallas_call | solution.py:207
  73.8 0.8 collective-permute-start.9
  74.6 5.5 %attend.7 = (f32[16,80,256]{2,1,0:T(8,128)S(1)}, f32[16,8,256]{2,1,0:T(8,128)S(1)}) custom-call(bf16[2,288,256]{2,1,0:T(8,128)(2,1)S(1)} %collective-permute-done.10.refs_0_, bf16[2,288,256]{2,1,0:T(8,128)(2,1)S(1)} %collective-permute-done.6.refs_1_, bf16[256,512]{1,0:T(8,128)(2,1)S(1)} %get-tuple-element.18.refs_2_.refs_3_, ...), custom_call_target="tpu_custom_call" | custom-call | flops 2818572288 | bytes 4194304 | tf_op jit(solution)/shard_map/attend/pallas_call | solution.py:207
  80.1 4.2 %attend.9 = bf16[12,80,256]{2,1,0:T(8,128)(2,1)S(1)} custom-call(bf16[2,288,256]{2,1,0:T(8,128)(2,1)S(1)} %collective-permute-done.7.refs_0_, bf16[1,288,256]{2,1,0:T(8,128)(2,1)S(1)} %collective-permute-done.8.refs_1_, bf16[1,288,256]{2,1,0:T(8,128)(2,1)S(1)} %collective-permute-done.9.refs_2_, bf16[256,512]{1,0:T(8,128)(2,1)S(1)} %get-tuple-element.18.refs_2_.refs_3_, ...), custom_call_target="tpu_custom_call" | custom-call | flops 2113929216 | bytes 4194304 | tf_op jit(solution)/shard_map/attend/pallas_call | solution.py:207
  84.4 2.6 %collective-permute-start.17 = (bf16[4,80,256]{2,1,0:T(8,128)(2,1)S(1)}, bf16[4,80,256]{2,1,0:T(8,128)(2,1)S(1)}, u32[]{:S(2)}, u32[]{:S(2)}) collective-permute-start(bf16[4,80,256]{2,1,0:T(8,128)(2,1)S(1)} %get-tuple-element.39), channel_id=1, source_target_pairs={{0,16},{4,20},{8,24},{12,28},{16,0},{20,4},{24,8},{28,12},{32,48},... | collective-permute-start | bytes 491528 | tf_op jit(solution)/shard_map/ppermute | solution.py:29
  87.0 0.7 collective-permute-start.16
  87.7 1.9 %collective-permute-start.15 = (bf16[4,80,256]{2,1,0:T(8,128)(2,1)S(1)}, bf16[4,80,256]{2,1,0:T(8,128)(2,1)S(1)}, u32[]{:S(2)}, u32[]{:S(2)}) collective-permute-start(bf16[4,80,256]{2,1,0:T(8,128)(2,1)S(1)} %get-tuple-element.41), channel_id=1, source_target_pairs={{0,24},{4,28},{8,0},{12,4},{16,8},{20,12},{24,16},{28,20},{32,56},... | collective-permute-start | bytes 491528 | tf_op jit(solution)/shard_map/ppermute | solution.py:29
  89.7 0.8 fusion.40.refs_5_
  90.5 2.0 %attend.8.refs_0_ = bf16[4,80,256]{2,1,0:T(8,128)(2,1)S(1)} custom-call(bf16[2,288,256]{2,1,0:T(8,128)(2,1)S(1)} %collective-permute-done.7.refs_0_, bf16[1,288,256]{2,1,0:T(8,128)(2,1)S(1)} %collective-permute-done.8.refs_1_, bf16[1,288,256]{2,1,0:T(8,128)(2,1)S(1)} %collective-permute-done.9.refs_2_, ...), custom_call_target="tpu_custom_call" | custom-call | flops 704643072 | bytes 4194304 | tf_op jit(solution)/shard_map/attend/pallas_call | solution.py:207
  92.6 3.1 %collective-permute-done.16.refs_2_ = bf16[4,80,256]{2,1,0:T(8,128)(2,1)S(1)} collective-permute-done((bf16[4,80,256]{2,1,0:T(8,128)(2,1)S(1)}, bf16[4,80,256]{2,1,0:T(8,128)(2,1)S(1)}, u32[]{:S(2)}, u32[]{:S(2)}) %collective-permute-start.16) | collective-permute-done | bytes 163872 | tf_op jit(solution)/shard_map/ppermute | solution.py:29
  96.2 1.0 collective-permute-start.25
  97.2 2.0 %collective-permute-start.26 = (bf16[256,512]{1,0:T(8,128)(2,1)S(1)}, bf16[256,512]{1,0:T(8,128)(2,1)S(1)}, u32[]{:S(2)}, u32[]{:S(2)}) collective-permute-start(bf16[256,512]{1,0:T(8,128)(2,1)S(1)} %get-tuple-element.29), channel_id=1, source_target_pairs={{0,2},{1,3},{2,0},{3,1},{4,6},{5,7},{6,4},{7,5},{8,10},{9,11},{10,... | collective-permute-start | bytes 786440 | tf_op jit(solution)/shard_map/ppermute | solution.py:43
  99.2 1.3 %collective-permute-start.27 = (bf16[256,512]{1,0:T(8,128)(2,1)S(1)}, bf16[256,512]{1,0:T(8,128)(2,1)S(1)}, u32[]{:S(2)}, u32[]{:S(2)}) collective-permute-start(bf16[256,512]{1,0:T(8,128)(2,1)S(1)} %get-tuple-element.30), channel_id=1, source_target_pairs={{0,3},{1,0},{2,1},{3,2},{4,7},{5,4},{6,5},{7,6},{8,11},{9,8},{10,9... | collective-permute-start | bytes 786440 | tf_op jit(solution)/shard_map/ppermute | solution.py:43
  100.5 4.1 %collective-permute-done.25 = bf16[256,512]{1,0:T(8,128)(2,1)S(1)} collective-permute-done((bf16[256,512]{1,0:T(8,128)(2,1)S(1)}, bf16[256,512]{1,0:T(8,128)(2,1)S(1)}, u32[]{:S(2)}, u32[]{:S(2)}) %collective-permute-start.25) | collective-permute-done | bytes 262176 | tf_op jit(solution)/shard_map/ppermute | solution.py:43
  104.6 5.8 %collective-permute-done.26 = bf16[256,512]{1,0:T(8,128)(2,1)S(1)} collective-permute-done((bf16[256,512]{1,0:T(8,128)(2,1)S(1)}, bf16[256,512]{1,0:T(8,128)(2,1)S(1)}, u32[]{:S(2)}, u32[]{:S(2)}) %collective-permute-start.26) | collective-permute-done | bytes 262176 | tf_op jit(solution)/shard_map/ppermute | solution.py:43
  110.9 0.8 add_convert_fusion
  (91 shorter events, 6.0 us)
Async XLA Ops:
  0.0 89.6 %copy-start = (bf16[512,2048]{1,0:T(8,128)(2,1)S(1)}, bf16[512,2048]{1,0:T(8,128)(2,1)}, u32[]{:S(2)}) copy-start(bf16[512,2048]{1,0:T(8,128)(2,1)} %param.35) | copy-start | bytes 6291460
  0.0 24.0 %copy-start.7 = (f32[2048]{0:T(1024)S(1)}, f32[2048]{0:T(1024)}, u32[]{:S(2)}) copy-start(f32[2048]{0:T(1024)} %param.19) | copy-start | bytes 24580
  0.0 18.5 %collective-permute-start.2 = (bf16[256,512]{1,0:T(8,128)(2,1)}, bf16[256,512]{1,0:T(8,128)(2,1)S(1)}, u32[]{:S(2)}, u32[]{:S(2)}) collective-permute-start(bf16[256,512]{1,0:T(8,128)(2,1)} %param.18), channel_id=1, source_target_pairs={{0,1},{1,2},{2,3},{3,0},{4,5},{5,6},{6,7},{7,4},{8,9},{9,10},{10,1... | collective-permute-start | bytes 786440 | tf_op jit(solution)/shard_map/ppermute | solution.py:43
  2.0 16.4 %collective-permute-start.1 = (bf16[256,512]{1,0:T(8,128)(2,1)}, bf16[256,512]{1,0:T(8,128)(2,1)S(1)}, u32[]{:S(2)}, u32[]{:S(2)}) collective-permute-start(bf16[256,512]{1,0:T(8,128)(2,1)} %param.18), channel_id=1, source_target_pairs={{0,2},{1,3},{2,0},{3,1},{4,6},{5,7},{6,4},{7,5},{8,10},{9,11},{10,... | collective-permute-start | bytes 786440 | tf_op jit(solution)/shard_map/ppermute | solution.py:43
  5.2 6.6 %collective-permute-start.18 = (bf16[16,512]{1,0:T(8,128)(2,1)S(1)}, bf16[16,512]{1,0:T(8,128)(2,1)S(1)}, u32[]{:S(2)}, u32[]{:S(2)}) collective-permute-start(bf16[16,512]{1,0:T(8,128)(2,1)S(1)} %get-tuple-element.42), channel_id=1, source_target_pairs={{4,8},{8,4},{12,16},{16,12},{20,24},{24,20},{28,32},{32,28},{36,40... | collective-permute-start | bytes 49160 | tf_op jit(solution)/shard_map/ppermute | solution.py:49
  9.6 2.3 %collective-permute-start.19 = (bf16[16,512]{1,0:T(8,128)(2,1)S(1)}, bf16[16,512]{1,0:T(8,128)(2,1)S(1)}, u32[]{:S(2)}, u32[]{:S(2)}) collective-permute-start(bf16[16,512]{1,0:T(8,128)(2,1)S(1)} %get-tuple-element.43), channel_id=1, source_target_pairs={{0,4},{4,0},{8,12},{12,8},{16,20},{20,16},{24,28},{28,24},{32,36},... | collective-permute-start | bytes 49160 | tf_op jit(solution)/shard_map/ppermute | solution.py:29
  11.9 4.8 %collective-permute-start.22 = (bf16[32,512]{1,0:T(8,128)(2,1)S(1)}, bf16[32,512]{1,0:T(8,128)(2,1)S(1)}, u32[]{:S(2)}, u32[]{:S(2)}) collective-permute-start(bf16[32,512]{1,0:T(8,128)(2,1)S(1)} %pad_maximum_fusion.8), channel_id=1, source_target_pairs={{0,1},{1,2},{2,3},{3,0},{4,5},{5,6},{6,7},{7,4},{8,9},{9,10},{10,1... | collective-permute-start | bytes 98312 | tf_op jit(solution)/shard_map/ppermute | solution.py:43
  12.0 5.4 %collective-permute-start.21 = (bf16[32,512]{1,0:T(8,128)(2,1)S(1)}, bf16[32,512]{1,0:T(8,128)(2,1)S(1)}, u32[]{:S(2)}, u32[]{:S(2)}) collective-permute-start(bf16[32,512]{1,0:T(8,128)(2,1)S(1)} %pad_maximum_fusion.8), channel_id=1, source_target_pairs={{0,2},{1,3},{2,0},{3,1},{4,6},{5,7},{6,4},{7,5},{8,10},{9,11},{10,... | collective-permute-start | bytes 98312 | tf_op jit(solution)/shard_map/ppermute | solution.py:43
  14.3 3.1 %collective-permute-start.20 = (bf16[32,512]{1,0:T(8,128)(2,1)S(1)}, bf16[32,512]{1,0:T(8,128)(2,1)S(1)}, u32[]{:S(2)}, u32[]{:S(2)}) collective-permute-start(bf16[32,512]{1,0:T(8,128)(2,1)S(1)} %pad_maximum_fusion.8), channel_id=1, source_target_pairs={{0,3},{1,0},{2,1},{3,2},{4,7},{5,4},{6,5},{7,6},{8,11},{9,8},{10,9... | collective-permute-start | bytes 98312 | tf_op jit(solution)/shard_map/ppermute | solution.py:43
  14.7 0.9 copy-start.2
  15.6 0.9 copy-start.3
  16.7 6.2 %collective-permute-start = (bf16[256,512]{1,0:T(8,128)(2,1)}, bf16[256,512]{1,0:T(8,128)(2,1)S(1)}, u32[]{:S(2)}, u32[]{:S(2)}) collective-permute-start(bf16[256,512]{1,0:T(8,128)(2,1)} %param.18), channel_id=1, source_target_pairs={{0,3},{1,0},{2,1},{3,2},{4,7},{5,4},{6,5},{7,6},{8,11},{9,8},{10,9... | collective-permute-start | bytes 786440 | tf_op jit(solution)/shard_map/ppermute | solution.py:43
  18.5 6.0 %copy-start.6 = (bf16[2048,32]{0,1:T(8,128)(2,1)S(1)}, bf16[2048,32]{0,1:T(8,128)(2,1)}, u32[]{:S(2)}) copy-start(bf16[2048,32]{0,1:T(8,128)(2,1)} %param.22) | copy-start | bytes 393220
  24.0 1.2 %copy-start.14 = (bf16[2048,256]{1,0:T(8,128)(2,1)S(1)}, bf16[2048,256]{1,0:T(8,128)(2,1)}, u32[]{:S(2)}) copy-start(bf16[2048,256]{1,0:T(8,128)(2,1)} %param.21) | copy-start | bytes 3145732
  24.4 1.5 %copy-start.10 = (f32[256]{0:T(256)S(1)}, f32[256]{0:T(256)}, u32[]{:S(2)}) copy-start(f32[256]{0:T(256)} %param.24) | copy-start | bytes 3076
  24.5 4.5 %copy-start.11 = (bf16[2048,512]{1,0:T(8,128)(2,1)S(1)}, bf16[2048,512]{1,0:T(8,128)(2,1)}, u32[]{:S(2)}) copy-start(bf16[2048,512]{1,0:T(8,128)(2,1)} %param.20) | copy-start | bytes 6291460
  26.1 3.7 %copy-start.5 = (bf16[512,128]{1,0:T(8,128)(2,1)S(1)}, bf16[512,128]{1,0:T(8,128)(2,1)}, u32[]{:S(2)}) copy-start(bf16[512,128]{1,0:T(8,128)(2,1)} %param.26) | copy-start | bytes 393220
  26.1 3.7 %copy-start.8 = (f32[512]{0:T(512)S(1)}, f32[512]{0:T(512)}, u32[]{:S(2)}) copy-start(f32[512]{0:T(512)} %param.23) | copy-start | bytes 6148
  26.1 4.0 %copy-start.4 = (bf16[512,256]{1,0:T(8,128)(2,1)S(1)}, bf16[512,256]{1,0:T(8,128)(2,1)}, u32[]{:S(2)}) copy-start(bf16[512,256]{1,0:T(8,128)(2,1)} %param.25) | copy-start | bytes 786436
  26.1 4.4 %copy-start.12 = (bf16[2048,512]{1,0:T(8,128)(2,1)S(1)}, bf16[2048,512]{1,0:T(8,128)(2,1)}, u32[]{:S(2)}) copy-start(bf16[2048,512]{1,0:T(8,128)(2,1)} %param.30) | copy-start | bytes 6291460
  26.1 10.9 %collective-permute-start.3 = (bf16[288,256]{1,0:T(8,128)(2,1)S(1)}, bf16[288,256]{1,0:T(8,128)(2,1)S(1)}, u32[]{:S(2)}, u32[]{:S(2)}) collective-permute-start(bf16[288,256]{1,0:T(8,128)(2,1)S(1)} %get-tuple-element.47), channel_id=1, source_target_pairs={{0,4},{4,0},{8,12},{12,8},{16,20},{20,16},{24,28},{28,24},{32,36},... | collective-permute-start | bytes 442376 | tf_op jit(solution)/shard_map/ppermute | solution.py:29
  30.6 1.6 %copy-start.13 = (bf16[2048,512]{1,0:T(8,128)(2,1)S(1)}, bf16[2048,512]{1,0:T(8,128)(2,1)}, u32[]{:S(2)}) copy-start(bf16[2048,512]{1,0:T(8,128)(2,1)} %param.29) | copy-start | bytes 6291460
  32.2 0.8 copy-start.9
  35.8 8.2 %collective-permute-start.23 = (f32[2,256]{1,0:T(2,128)S(1)}, f32[2,256]{1,0:T(2,128)S(1)}, u32[]{:S(2)}, u32[]{:S(2)}) collective-permute-start(f32[2,256]{1,0:T(2,128)S(1)} %pad_maximum_fusion.9), channel_id=1, source_target_pairs={{0,1},{1,0},{2,3},{3,2},{4,5},{5,4},{6,7},{7,6},{8,9},{9,8},{10,11... | collective-permute-start | bytes 6152 | tf_op jit(solution)/shard_map/ppermute | solution.py:401
  37.1 10.6 %collective-permute-start.4 = (bf16[2,288,256]{2,1,0:T(8,128)(2,1)S(1)}, bf16[2,288,256]{2,1,0:T(8,128)(2,1)S(1)}, u32[]{:S(2)}, u32[]{:S(2)}) collective-permute-start(bf16[2,288,256]{2,1,0:T(8,128)(2,1)S(1)} %pad_maximum_fusion.4.refs_0_), channel_id=1, source_target_pairs={{0,32},{4,228},{8,40},{12,236},{16,48},{20,244},{24,56},{28,252},{... | collective-permute-start | bytes 884744 | tf_op jit(solution)/shard_map/ppermute | solution.py:38
  44.1 10.3 %collective-permute-start.24 = (f32[2,256]{1,0:T(2,128)S(1)}, f32[2,256]{1,0:T(2,128)S(1)}, u32[]{:S(2)}, u32[]{:S(2)}) collective-permute-start(f32[2,256]{1,0:T(2,128)S(1)} %pad_maximum_fusion.10), channel_id=1, source_target_pairs={{0,2},{1,3},{2,0},{3,1},{4,6},{5,7},{6,4},{7,5},{8,10},{9,11},{10,... | collective-permute-start | bytes 6152 | tf_op jit(solution)/shard_map/ppermute | solution.py:401
  47.7 7.0 %collective-permute-start.5 = (bf16[2,288,256]{2,1,0:T(8,128)(2,1)S(1)}, bf16[2,288,256]{2,1,0:T(8,128)(2,1)S(1)}, u32[]{:S(2)}, u32[]{:S(2)}) collective-permute-start(bf16[2,288,256]{2,1,0:T(8,128)(2,1)S(1)} %collective-permute-done.4.refs_1_), channel_id=1, source_target_pairs={{0,32},{4,228},{8,40},{12,236},{16,48},{20,244},{24,56},{28,252},{... | collective-permute-start | bytes 884744 | tf_op jit(solution)/shard_map/ppermute | solution.py:38
  51.0 8.2 %collective-permute-start.13 = (bf16[384,256]{1,0:T(8,128)(2,1)S(1)}, bf16[384,256]{1,0:T(8,128)(2,1)S(1)}, u32[]{:S(2)}, u32[]{:S(2)}) collective-permute-start(bf16[384,256]{1,0:T(8,128)(2,1)S(1)} %bitcast.66), channel_id=1, source_target_pairs={{0,16},{4,20},{8,24},{12,28},{16,0},{20,4},{24,8},{28,12},{32,48},... | collective-permute-start | bytes 589832 | tf_op jit(solution)/shard_map/ppermute | solution.py:29
  52.9 9.0 %collective-permute-start.12 = (bf16[384,256]{1,0:T(8,128)(2,1)S(1)}, bf16[384,256]{1,0:T(8,128)(2,1)S(1)}, u32[]{:S(2)}, u32[]{:S(2)}) collective-permute-start(bf16[384,256]{1,0:T(8,128)(2,1)S(1)} %bitcast.67), channel_id=1, source_target_pairs={{0,24},{4,28},{8,0},{12,4},{16,8},{20,12},{24,16},{28,20},{32,56},... | collective-permute-start | bytes 589832 | tf_op jit(solution)/shard_map/ppermute | solution.py:29
  53.7 8.8 %collective-permute-start.11 = (bf16[384,256]{1,0:T(8,128)(2,1)S(1)}, bf16[384,256]{1,0:T(8,128)(2,1)S(1)}, u32[]{:S(2)}, u32[]{:S(2)}) collective-permute-start(bf16[384,256]{1,0:T(8,128)(2,1)S(1)} %bitcast.68), channel_id=1, source_target_pairs={{0,8},{4,12},{8,16},{12,20},{16,24},{20,28},{24,0},{28,4},{32,40},... | collective-permute-start | bytes 589832 | tf_op jit(solution)/shard_map/ppermute | solution.py:29
  54.3 14.0 %collective-permute-start.14 = (bf16[2,288,256]{2,1,0:T(8,128)(2,1)S(1)}, bf16[2,288,256]{2,1,0:T(8,128)(2,1)S(1)}, u32[]{:S(2)}, u32[]{:S(2)}) collective-permute-start(bf16[2,288,256]{2,1,0:T(8,128)(2,1)S(1)} %collective-permute-done.4.refs_1_), channel_id=1, source_target_pairs={{0,4},{4,0},{8,12},{12,8},{16,20},{20,16},{24,28},{28,24},{32,36},... | collective-permute-start | bytes 884744 | tf_op jit(solution)/shard_map/ppermute | solution.py:29
  54.7 13.3 %collective-permute-start.6 = (bf16[2,288,256]{2,1,0:T(8,128)(2,1)S(1)}, bf16[2,288,256]{2,1,0:T(8,128)(2,1)S(1)}, u32[]{:S(2)}, u32[]{:S(2)}) collective-permute-start(bf16[2,288,256]{2,1,0:T(8,128)(2,1)S(1)} %collective-permute-done.5.refs_1_), channel_id=1, source_target_pairs={{0,32},{4,228},{8,40},{12,236},{16,48},{20,244},{24,56},{28,252},{... | collective-permute-start | bytes 884744 | tf_op jit(solution)/shard_map/ppermute | solution.py:38
  59.3 15.3 %collective-permute-start.10 = (bf16[2,288,256]{2,1,0:T(8,128)(2,1)S(1)}, bf16[2,288,256]{2,1,0:T(8,128)(2,1)S(1)}, u32[]{:S(2)}, u32[]{:S(2)}) collective-permute-start(bf16[2,288,256]{2,1,0:T(8,128)(2,1)S(1)} %collective-permute-done.5.refs_1_), channel_id=1, source_target_pairs={{0,4},{4,0},{8,12},{12,8},{16,20},{20,16},{24,28},{28,24},{32,36},... | collective-permute-start | bytes 884744 | tf_op jit(solution)/shard_map/ppermute | solution.py:29
  68.0 5.8 %collective-permute-start.8 = (bf16[1,288,256]{2,1,0:T(8,128)(2,1)S(1)}, bf16[1,288,256]{2,1,0:T(8,128)(2,1)S(1)}, u32[]{:S(2)}, u32[]{:S(2)}) collective-permute-start(bf16[1,288,256]{2,1,0:T(8,128)(2,1)S(1)} %slice.367), channel_id=1, source_target_pairs={{0,32},{4,228},{8,40},{12,236},{16,48},{20,244},{24,56},{28,252},{... | collective-permute-start | bytes 442376 | tf_op jit(solution)/shard_map/ppermute | solution.py:38
  68.2 11.8 %collective-permute-start.7 = (bf16[2,288,256]{2,1,0:T(8,128)(2,1)S(1)}, bf16[2,288,256]{2,1,0:T(8,128)(2,1)S(1)}, u32[]{:S(2)}, u32[]{:S(2)}) collective-permute-start(bf16[2,288,256]{2,1,0:T(8,128)(2,1)S(1)} %collective-permute-done.6.refs_1_), channel_id=1, source_target_pairs={{0,4},{4,0},{8,12},{12,8},{16,20},{20,16},{24,28},{28,24},{32,36},... | collective-permute-start | bytes 884744 | tf_op jit(solution)/shard_map/ppermute | solution.py:29
  73.8 6.3 %collective-permute-start.9 = (bf16[1,288,256]{2,1,0:T(8,128)(2,1)S(1)}, bf16[1,288,256]{2,1,0:T(8,128)(2,1)S(1)}, u32[]{:S(2)}, u32[]{:S(2)}) collective-permute-start(bf16[1,288,256]{2,1,0:T(8,128)(2,1)S(1)} %collective-permute-done.8.refs_1_), channel_id=1, source_target_pairs={{0,4},{4,0},{8,12},{12,8},{16,20},{20,16},{24,28},{28,24},{32,36},... | collective-permute-start | bytes 442376 | tf_op jit(solution)/shard_map/ppermute | solution.py:29
  80.1 9.6 %copy-start.15 = (f32[512]{0:T(512)S(1)}, f32[512]{0:T(512)}, u32[]{:S(2)}) copy-start(f32[512]{0:T(512)} %param.33) | copy-start | bytes 6148
  84.4 8.2 %collective-permute-start.17 = (bf16[4,80,256]{2,1,0:T(8,128)(2,1)S(1)}, bf16[4,80,256]{2,1,0:T(8,128)(2,1)S(1)}, u32[]{:S(2)}, u32[]{:S(2)}) collective-permute-start(bf16[4,80,256]{2,1,0:T(8,128)(2,1)S(1)} %get-tuple-element.39), channel_id=1, source_target_pairs={{0,16},{4,20},{8,24},{12,28},{16,0},{20,4},{24,8},{28,12},{32,48},... | collective-permute-start | bytes 491528 | tf_op jit(solution)/shard_map/ppermute | solution.py:29
  87.0 8.7 %collective-permute-start.16 = (bf16[4,80,256]{2,1,0:T(8,128)(2,1)S(1)}, bf16[4,80,256]{2,1,0:T(8,128)(2,1)S(1)}, u32[]{:S(2)}, u32[]{:S(2)}) collective-permute-start(bf16[4,80,256]{2,1,0:T(8,128)(2,1)S(1)} %get-tuple-element.40), channel_id=1, source_target_pairs={{0,8},{4,12},{8,16},{12,20},{16,24},{20,28},{24,0},{28,4},{32,40},... | collective-permute-start | bytes 491528 | tf_op jit(solution)/shard_map/ppermute | solution.py:29
  87.7 7.9 %collective-permute-start.15 = (bf16[4,80,256]{2,1,0:T(8,128)(2,1)S(1)}, bf16[4,80,256]{2,1,0:T(8,128)(2,1)S(1)}, u32[]{:S(2)}, u32[]{:S(2)}) collective-permute-start(bf16[4,80,256]{2,1,0:T(8,128)(2,1)S(1)} %get-tuple-element.41), channel_id=1, source_target_pairs={{0,24},{4,28},{8,0},{12,4},{16,8},{20,12},{24,16},{28,20},{32,56},... | collective-permute-start | bytes 491528 | tf_op jit(solution)/shard_map/ppermute | solution.py:29
  90.5 5.1 %copy-start.1 = (bf16[256,2048]{1,0:T(8,128)(2,1)S(1)}, bf16[256,2048]{1,0:T(8,128)(2,1)}, u32[]{:S(2)}) copy-start(bf16[256,2048]{1,0:T(8,128)(2,1)} %refs_4_.1) | copy-start | bytes 3145732
  96.2 8.4 %collective-permute-start.25 = (bf16[256,512]{1,0:T(8,128)(2,1)S(1)}, bf16[256,512]{1,0:T(8,128)(2,1)S(1)}, u32[]{:S(2)}, u32[]{:S(2)}) collective-permute-start(bf16[256,512]{1,0:T(8,128)(2,1)S(1)} %get-tuple-element.28), channel_id=1, source_target_pairs={{0,1},{1,2},{2,3},{3,0},{4,5},{5,6},{6,7},{7,4},{8,9},{9,10},{10,1... | collective-permute-start | bytes 786440 | tf_op jit(solution)/shard_map/ppermute | solution.py:43
  97.2 13.2 %collective-permute-start.26 = (bf16[256,512]{1,0:T(8,128)(2,1)S(1)}, bf16[256,512]{1,0:T(8,128)(2,1)S(1)}, u32[]{:S(2)}, u32[]{:S(2)}) collective-permute-start(bf16[256,512]{1,0:T(8,128)(2,1)S(1)} %get-tuple-element.29), channel_id=1, source_target_pairs={{0,2},{1,3},{2,0},{3,1},{4,6},{5,7},{6,4},{7,5},{8,10},{9,11},{10,... | collective-permute-start | bytes 786440 | tf_op jit(solution)/shard_map/ppermute | solution.py:43
  99.2 11.7 %collective-permute-start.27 = (bf16[256,512]{1,0:T(8,128)(2,1)S(1)}, bf16[256,512]{1,0:T(8,128)(2,1)S(1)}, u32[]{:S(2)}, u32[]{:S(2)}) collective-permute-start(bf16[256,512]{1,0:T(8,128)(2,1)S(1)} %get-tuple-element.30), channel_id=1, source_target_pairs={{0,3},{1,0},{2,1},{3,2},{4,7},{5,4},{6,5},{7,6},{8,11},{9,8},{10,9... | collective-permute-start | bytes 786440 | tf_op jit(solution)/shard_map/ppermute | solution.py:43
